TPU v7x, 512 devices: a whole 4x4x16 slice. The times are simulated.
512 devices in a mesh: rep: 2 (over z_hi), fs: 32 (over z_lo, y), tp: 8 (over x, core).
Axes of the slice: x: 4, y: 4, z: 16 (z_hi: 2, z_lo: 8; z = z_hi * 8 + z_lo), core: 2. Of those that a mesh axis runs over, the one named last changes fastest.
Arguments:
- stream: bfloat16 [24576, 2048], P(('rep', 'fs'), 'tp'), may hold values from -24 to 24
- recurrence_input_weight: bfloat16 [2048, 2048], P('fs', 'tp'), may hold values from -0.125 to 0.125
- output_gate_weight: bfloat16 [2048, 2048], P('fs', 'tp'), may hold values from -0.125 to 0.125
- recurrence_gate_matrix: bfloat16 [16, 128, 128], P('tp'), may hold values from -0.5 to 0.5
- input_gate_matrix: bfloat16 [16, 128, 128], P('tp'), may hold values from -0.5 to 0.5
- channel_decay_rate: float32 [2048], P('tp')
- recurrence_taps: float32 [4, 2048], P(None, 'tp'), may hold values from -3 to 3
- spike_log_decay: float32 [24576, 16], P(('rep', 'fs'), 'tp'), may hold values from -2.1 to 0
- recurrence_output_weight: bfloat16 [2048, 2048], P('tp', 'fs'), may hold values from -0.3125 to 0.3125
- feedforward_gate_upward: bfloat16 [2048, 4096], P('fs', 'tp'), may hold values from -0.125 to 0.125
- feedforward_value_upward: bfloat16 [2048, 4096], P('fs', 'tp'), may hold values from -0.125 to 0.125
- feedforward_gate_taps: float32 [3, 4096], P(None, 'tp'), may hold values from -3 to 3
- feedforward_value_taps: float32 [3, 4096], P(None, 'tp'), may hold values from -3 to 3
- feedforward_down_weight: bfloat16 [4096, 2048], P('tp', 'fs'), may hold values from -0.1875 to 0.1875
- recurrence_norm_gain: float32 [2048], replicated, may hold values from 0.1 to 1.9
- feedforward_norm_gain: float32 [2048], replicated, may hold values from 0.1 to 1.9
- closing_norm_gain: float32 [2048], replicated, may hold values from 0.1 to 1.9
Outputs:
- layer_out: bfloat16 [24576, 2048], P(('rep', 'fs'), 'tp')
All inputs are finite; a program needn't handle non-finite values.
Results may differ from a plain program's by a relative error of at most 0.018.
Values may be sent and summed in bfloat16 or wider, within the bound.
A program may use at most 64 MiB of HBM per device.

v0:
```python
import jax
import jax.numpy as jnp
from jax import lax
from jax.sharding import PartitionSpec as P

EPS = 1e-06
GATE_POWER = 8.0


def in_one_piece(arrays, axis, dim, along):
    ends, at = ([], 0)
    for a in arrays[:-1]:
        at += a.shape[along]
        ends.append(at)
    both = jnp.concatenate(arrays, axis=along)
    return tuple(jnp.split(lax.all_gather(both, axis, axis=dim, tiled=True), ends, axis=along))


def in_order(pieces, dim):
    pieces = jnp.moveaxis(pieces, 0, dim)
    lengths = pieces.shape
    return pieces.reshape(*lengths[:dim], lengths[dim] * lengths[dim + 1], *lengths[dim + 2 :])


def from_everyone(shard, axis):
    copies = jnp.broadcast_to(shard, (lax.axis_size(axis), *shard.shape))
    return lax.all_to_all(copies, axis, split_axis=0, concat_axis=0, tiled=True)


def gathered_copies(shard, axis, dim):
    return in_order(from_everyone(shard, axis), dim)


def cut_along(shard, dim, peers):
    lengths = shard.shape
    pieces = shard.reshape(*lengths[:dim], peers, lengths[dim] // peers, *lengths[dim + 1 :])
    return jnp.moveaxis(pieces, dim, 0)


def sent_and_summed(shard, axis, dim):
    peers = lax.axis_size(axis)
    pieces = lax.all_to_all(cut_along(shard, dim, peers), axis, 0, 0, tiled=True)
    return jnp.sum(pieces.astype(jnp.float32), axis=0)


def over_copies(shard, axis):
    everything = from_everyone(shard, axis)
    return jnp.sum(everything, axis=0)


def rms_scale(row_block, gain_vec):
    widened = row_block.astype(jnp.float32)
    inverse = lax.rsqrt(jnp.mean(widened * widened, axis=-1, keepdims=True) + EPS)
    return (widened * inverse * gain_vec).astype(jnp.bfloat16)


def causal_mix(values, kernel_taps):
    extent = kernel_taps.shape[0]
    length = values.shape[0]
    padded = jnp.pad(values, ((extent - 1, 0), (0, 0)))
    summed = kernel_taps[0] * padded[0:length]
    for offset in range(1, extent):
        summed = summed + kernel_taps[offset] * padded[offset : offset + length]
    return summed


def chain_step(earlier, following):
    return (earlier[0] * following[0], following[0] * earlier[1] + following[1])


def fold_pair(source, pieces):
    return (
        jnp.dot(source, pieces[0], preferred_element_type=jnp.float32),
        jnp.dot(source, pieces[1], preferred_element_type=jnp.float32),
    )


def project_with(left_rows, weight_piece):
    return jnp.dot(left_rows, weight_piece, preferred_element_type=jnp.float32).astype(jnp.bfloat16)


def shards(
    stream,
    recurrence_input_weight,
    output_gate_weight,
    recurrence_gate_matrix,
    input_gate_matrix,
    channel_decay_rate,
    recurrence_taps,
    spike_log_decay,
    recurrence_output_weight,
    feedforward_gate_upward,
    feedforward_value_upward,
    feedforward_gate_taps,
    feedforward_value_taps,
    feedforward_down_weight,
    recurrence_norm_gain,
    feedforward_norm_gain,
    closing_norm_gain,
):
    collected = in_one_piece((feedforward_gate_upward, feedforward_value_upward), "fs", 0, 1)
    tok_rows = stream.shape[0]
    head_count = recurrence_gate_matrix.shape[0]
    block_size = recurrence_gate_matrix.shape[1]
    whole_rows = gathered_copies(stream, "tp", 1)
    normed = rms_scale(whole_rows, recurrence_norm_gain)
    rec_sum, gate_sum = fold_pair(
        normed, in_one_piece((recurrence_input_weight, output_gate_weight), "fs", 0, 1)
    )
    rec_in = rec_sum.astype(jnp.bfloat16)
    gate_src = gate_sum.astype(jnp.bfloat16)
    conv_out = causal_mix(rec_in.astype(jnp.float32), recurrence_taps).astype(jnp.bfloat16)
    blocks = conv_out.reshape(tok_rows, head_count, block_size)
    gate_restart = jax.nn.sigmoid(
        jnp.einsum(
            "thi,hij->thj", blocks, recurrence_gate_matrix, preferred_element_type=jnp.float32
        )
    )
    admit_gate = jax.nn.sigmoid(
        jnp.einsum("thi,hij->thj", blocks, input_gate_matrix, preferred_element_type=jnp.float32)
    )
    decay_base = (GATE_POWER * jax.nn.softplus(-channel_decay_rate)).reshape(head_count, block_size)
    decay_logarithm = -gate_restart * decay_base + spike_log_decay[:, :, None]
    decay_rate = jnp.exp(decay_logarithm)
    inflow = jnp.sqrt(-jnp.expm1(2.0 * decay_logarithm)) * admit_gate * blocks.astype(jnp.float32)
    states = lax.associative_scan(chain_step, (decay_rate, inflow), axis=0)[1]
    mixed_out = (
        states.reshape(tok_rows, head_count * block_size)
        * jax.nn.gelu(gate_src.astype(jnp.float32))
    ).astype(jnp.bfloat16)
    mix_terms = project_with(mixed_out, gathered_copies(recurrence_output_weight, "fs", 1))
    branch = sent_and_summed(
        lax.optimization_barrier(mix_terms).astype(jnp.float32).astype(jnp.bfloat16), "tp", 1
    ).astype(jnp.bfloat16)
    middle = (stream.astype(jnp.float32) + branch.astype(jnp.float32)).astype(jnp.bfloat16)
    whole_middle = gathered_copies(middle, "tp", 1)
    normed_ffn = rms_scale(whole_middle, feedforward_norm_gain)
    gate_sum_ffn = jnp.dot(normed_ffn, collected[0], preferred_element_type=jnp.float32)
    value_sum_ffn = jnp.dot(normed_ffn, collected[1], preferred_element_type=jnp.float32)
    gate_up = gate_sum_ffn.astype(jnp.bfloat16)
    value_up = value_sum_ffn.astype(jnp.bfloat16)
    gate_conv = causal_mix(gate_up.astype(jnp.float32), feedforward_gate_taps)
    value_conv = causal_mix(value_up.astype(jnp.float32), feedforward_value_taps)
    hidden = (jax.nn.gelu(gate_conv) * value_conv).astype(jnp.bfloat16)
    down_terms = project_with(hidden, gathered_copies(feedforward_down_weight, "fs", 1))
    branch_ffn = sent_and_summed(
        lax.optimization_barrier(down_terms).astype(jnp.float32).astype(jnp.bfloat16), "tp", 1
    ).astype(jnp.bfloat16)
    final_rows = middle.astype(jnp.float32) + branch_ffn.astype(jnp.float32)
    col_count = final_rows.shape[1]
    square_sum = over_copies(jnp.sum(final_rows * final_rows, axis=1), "tp")
    inverse = lax.rsqrt(square_sum / (col_count * lax.axis_size("tp")) + EPS)
    gain_part = lax.dynamic_slice_in_dim(
        closing_norm_gain, lax.axis_index("tp") * col_count, col_count
    )
    return (final_rows * inverse[:, None] * gain_part[None, :]).astype(jnp.bfloat16)


def solution(mesh):
    in_specs = (
        P(("rep", "fs"), "tp"),
        P("fs", "tp"),
        P("fs", "tp"),
        P("tp", None, None),
        P("tp", None, None),
        P("tp"),
        P(None, "tp"),
        P(("rep", "fs"), "tp"),
        P("tp", "fs"),
        P("fs", "tp"),
        P("fs", "tp"),
        P(None, "tp"),
        P(None, "tp"),
        P("tp", "fs"),
        P(),
        P(),
        P(),
    )
    out_specs = P(("rep", "fs"), "tp")
    return jax.shard_map(shards, mesh=mesh, in_specs=in_specs, out_specs=out_specs, check_vma=False)
```

profile of v0, /device:TPU:1, one launch (start us, length us, event | category | flops | bytes accessed | tf_op | source)
XLA Modules:
  0.0 580.8 jit_solution(769760791556727926)
XLA Ops:
  6.5 1.4 pad_maximum_fusion.3
  8.0 1.1 copy.48
  9.1 1.3 broadcast_in_dim.10
  10.4 10.3 %all-to-all-start = ((bf16[8,384,256]{1,2,0:T(8,128)(2,1)}), bf16[8,384,256]{1,2,0:T(8,128)(2,1)S(1)}, u32[]{:S(2)}, u32[]{:S(2)}) async-start(bf16[8,384,256]{1,2,0:T(8,128)(2,1)} %broadcast_in_dim.10), calls=%async_computation | async-start | bytes 3145728 | tf_op jit(solution)/shard_map/all_to_all | solution.py:27
  20.8 20.7 %all-to-all-done = bf16[8,384,256]{1,2,0:T(8,128)(2,1)S(1)} async-done(((bf16[8,384,256]{1,2,0:T(8,128)(2,1)}), bf16[8,384,256]{1,2,0:T(8,128)(2,1)S(1)}, u32[]{:S(2)}, u32[]{:S(2)}) %all-to-all-start) | async-done | bytes 1572896 | tf_op jit(solution)/shard_map/all_to_all | solution.py:27
  41.4 1.1 broadcast_in_dim.11
  42.5 10.9 %all-to-all-start.1 = ((bf16[32,256,64]{1,2,0:T(8,128)(2,1)}), bf16[32,256,64]{1,2,0:T(8,128)(2,1)}, u32[]{:S(2)}, u32[]{:S(2)}) async-start(bf16[32,256,64]{1,2,0:T(8,128)(2,1)} %broadcast_in_dim.11), calls=%async_computation.1 | async-start | bytes 2097152 | tf_op jit(solution)/shard_map/all_to_all | solution.py:27
  54.3 163.4 %all-gather.3.cloned.1.call-done = bf16[2048,512]{1,0:T(8,128)(2,1)} async-done(((bf16[64,512]{1,0:T(8,128)(2,1)}), bf16[2048,512]{1,0:T(8,128)(2,1)}) %all-gather.3.cloned.1.call-update) | async-done | bytes 2097168 | tf_op jit(solution)/shard_map/all_gather | solution.py:16
  217.7 1.8 fusion.34
  220.9 0.7 slice.256
  221.6 1.0 fusion.104
  223.1 0.6 slice.289
  223.7 0.6 slice.290
  224.3 0.6 slice.288
  224.9 0.6 slice.292
  226.1 0.6 slice.298
  227.2 0.6 slice.281
  227.8 0.6 slice.300
  229.0 0.6 slice.275
  229.6 0.6 slice.302
  233.4 0.7 fusion.112
  234.2 0.7 fusion.92
  234.9 0.6 pad_maximum_fusion.8
  235.5 0.7 fusion.89
  236.3 0.7 pad_maximum_fusion.7
  237.0 0.7 fusion.88
  237.7 0.7 pad_maximum_fusion.6
  238.5 0.7 pad_maximum_fusion.5
  240.2 0.9 copy.53
  241.1 3.5 convolution_convert_fusion.1
  244.8 46.7 %all_to_all.36 = bf16[8,384,256]{2,1,0:T(8,128)(2,1)S(1)} all-to-all(bf16[8,384,256]{2,1,0:T(8,128)(2,1)S(1)} %bitcast.76), channel_id=1, replica_groups=mesh['rep'=2,'fs'=32,'tp'=8] {'tp'}, dimensions={0} | all-to-all | bytes 3145728 | tf_op jit(solution)/shard_map/all_to_all | solution.py:42
  291.8 1.0 add_convert_fusion
  292.9 1.3 broadcast_in_dim.24
  294.2 4.7 all-to-all-start.3
  298.9 0.7 pad_maximum_fusion.1
  299.6 19.9 %all-to-all-done.3 = bf16[8,384,256]{1,2,0:T(8,128)(2,1)S(1)} async-done(((bf16[8,384,256]{1,2,0:T(8,128)(2,1)}), bf16[8,384,256]{1,2,0:T(8,128)(2,1)S(1)}, u32[]{:S(2)}, u32[]{:S(2)}) %all-to-all-start.3) | async-done | bytes 1572896 | tf_op jit(solution)/shard_map/all_to_all | solution.py:27
  319.5 1.6 broadcast_in_dim.25
  321.2 12.2 %all-to-all-start.4 = ((bf16[32,512,64]{1,2,0:T(8,128)(2,1)}), bf16[32,512,64]{1,2,0:T(8,128)(2,1)}, u32[]{:S(2)}, u32[]{:S(2)}) async-start(bf16[32,512,64]{1,2,0:T(8,128)(2,1)} %broadcast_in_dim.25), calls=%async_computation.4 | async-start | bytes 4194304 | tf_op jit(solution)/shard_map/all_to_all | solution.py:27
  334.2 175.3 %all-gather.5.cloned.1.call-done = bf16[2048,1024]{1,0:T(8,128)(2,1)} async-done(((bf16[64,1024]{1,0:T(8,128)(2,1)}), bf16[2048,1024]{1,0:T(8,128)(2,1)}) %all-gather.5.cloned.1.call-update) | async-done | bytes 4194320 | tf_op jit(solution)/shard_map/all_gather | solution.py:16
  509.6 2.7 fusion.11
  512.4 1.0 fusion.17
  513.4 3.1 convolution_convert_fusion
  516.7 46.5 %all_to_all.37 = bf16[8,384,256]{2,1,0:T(8,128)(2,1)S(1)} all-to-all(bf16[8,384,256]{2,1,0:T(8,128)(2,1)S(1)} %bitcast.77), channel_id=1, replica_groups=mesh['rep'=2,'fs'=32,'tp'=8] {'tp'}, dimensions={0} | all-to-all | bytes 3145728 | tf_op jit(solution)/shard_map/all_to_all | solution.py:42
  563.6 0.6 broadcast_in_dim.26
  564.2 4.3 all-to-all-start.6
  568.5 0.8 dynamic_slice.3
  569.3 3.9 all-to-all-done.6
  573.2 0.8 multiply_convert_fusion
  (138 shorter events, 10.6 us)
Async XLA Ops:
  6.5 213.2 %copy-start = (bf16[2,128,128]{2,1,0:T(8,128)(2,1)S(1)}, bf16[2,128,128]{2,1,0:T(8,128)(2,1)}, u32[]{:S(2)}) copy-start(bf16[2,128,128]{2,1,0:T(8,128)(2,1)} %param.20) | copy-start | bytes 196612
  6.5 211.2 %all-gather.3.cloned.1.call-start = ((), (), s32[]{:S(2)}) async-start(), calls=%async_computation.7 | async-start | bytes 2162688 | tf_op jit(solution)/shard_map/all_gather | solution.py:16
  9.1 11.6 %copy-start.14 = (f32[256]{0:T(256)S(1)}, f32[256]{0:T(256)}, u32[]{:S(2)}) copy-start(f32[256]{0:T(256)} %param.22) | copy-start | bytes 3076
  9.1 11.6 %copy-start.13 = (f32[4,256]{1,0:T(4,128)S(1)}, f32[4,256]{1,0:T(4,128)}, u32[]{:S(2)}) copy-start(f32[4,256]{1,0:T(4,128)} %param.23) | copy-start | bytes 12292
  9.1 32.3 %copy-start.5 = (bf16[256,64]{0,1:T(8,128)(2,1)S(1)}, bf16[256,64]{0,1:T(8,128)(2,1)}, u32[]{:S(2)}) copy-start(bf16[256,64]{0,1:T(8,128)(2,1)} %param.25) | copy-start | bytes 98308
  10.4 31.0 %all-to-all-start = ((bf16[8,384,256]{1,2,0:T(8,128)(2,1)}), bf16[8,384,256]{1,2,0:T(8,128)(2,1)S(1)}, u32[]{:S(2)}, u32[]{:S(2)}) async-start(bf16[8,384,256]{1,2,0:T(8,128)(2,1)} %broadcast_in_dim.10), calls=%async_computation | async-start | bytes 3145728 | tf_op jit(solution)/shard_map/all_to_all | solution.py:27
  42.5 11.3 %copy-start.6 = (f32[2048]{0:T(1024)S(1)}, f32[2048]{0:T(1024)}, u32[]{:S(2)}) copy-start(f32[2048]{0:T(1024)} %param.31) | copy-start | bytes 24580
  42.5 198.6 %all-to-all-start.1 = ((bf16[32,256,64]{1,2,0:T(8,128)(2,1)}), bf16[32,256,64]{1,2,0:T(8,128)(2,1)}, u32[]{:S(2)}, u32[]{:S(2)}) async-start(bf16[32,256,64]{1,2,0:T(8,128)(2,1)} %broadcast_in_dim.11), calls=%async_computation.1 | async-start | bytes 2097152 | tf_op jit(solution)/shard_map/all_to_all | solution.py:27
  54.2 165.5 %copy-start.16 = (f32[384,2]{0,1:T(2,128)S(1)}, f32[384,2]{0,1:T(2,128)}, u32[]{:S(2)}) copy-start(f32[384,2]{0,1:T(2,128)} %param.24) | copy-start | bytes 9220
  219.5 0.8 copy-start.15
  232.1 7.2 %copy-start.12 = (f32[1,2,128]{2,0,1:T(1,128)S(1)}, f32[1,2,128]{2,0,1:T(1,128)}, u32[]{:S(2)}) copy-start(f32[1,2,128]{2,0,1:T(1,128)} %slice.323) | copy-start | bytes 3076
  232.8 6.6 %copy-start.11 = (f32[1,2,128]{2,0,1:T(1,128)S(1)}, f32[1,2,128]{2,0,1:T(1,128)}, u32[]{:S(2)}) copy-start(f32[1,2,128]{2,0,1:T(1,128)} %slice.322) | copy-start | bytes 3076
  239.2 0.7 copy-start.10
  292.9 6.0 %copy-start.3 = (bf16[64,512]{1,0:T(8,128)(2,1)S(1)}, bf16[64,512]{1,0:T(8,128)(2,1)}, u32[]{:S(2)}) copy-start(bf16[64,512]{1,0:T(8,128)(2,1)} %param.27) | copy-start | bytes 196612
  292.9 6.0 %copy-start.4 = (bf16[64,512]{1,0:T(8,128)(2,1)S(1)}, bf16[64,512]{1,0:T(8,128)(2,1)}, u32[]{:S(2)}) copy-start(bf16[64,512]{1,0:T(8,128)(2,1)} %param.26) | copy-start | bytes 196612
  294.2 25.3 %copy-start.2 = (bf16[512,64]{0,1:T(8,128)(2,1)S(1)}, bf16[512,64]{0,1:T(8,128)(2,1)}, u32[]{:S(2)}) copy-start(bf16[512,64]{0,1:T(8,128)(2,1)} %param.30) | copy-start | bytes 196612
  294.2 25.3 %all-to-all-start.3 = ((bf16[8,384,256]{1,2,0:T(8,128)(2,1)}), bf16[8,384,256]{1,2,0:T(8,128)(2,1)S(1)}, u32[]{:S(2)}, u32[]{:S(2)}) async-start(bf16[8,384,256]{1,2,0:T(8,128)(2,1)} %broadcast_in_dim.24), calls=%async_computation.3 | async-start | bytes 3145728 | tf_op jit(solution)/shard_map/all_to_all | solution.py:27
  298.9 210.7 %all-gather.5.cloned.1.call-start = ((), (), s32[]{:S(2)}) async-start(), calls=%async_computation.8 | async-start | bytes 4325376 | tf_op jit(solution)/shard_map/all_gather | solution.py:16
  321.2 12.2 %copy-start.8 = (f32[3,512]{1,0:T(4,128)S(1)}, f32[3,512]{1,0:T(4,128)}, u32[]{:S(2)}) copy-start(f32[3,512]{1,0:T(4,128)} %param.28) | copy-start | bytes 18436
  321.2 12.2 %copy-start.9 = (f32[3,512]{1,0:T(4,128)S(1)}, f32[3,512]{1,0:T(4,128)}, u32[]{:S(2)}) copy-start(f32[3,512]{1,0:T(4,128)} %param.29) | copy-start | bytes 18436
  321.2 12.7 %copy-start.7 = (f32[2048]{0:T(1024)S(1)}, f32[2048]{0:T(1024)}, u32[]{:S(2)}) copy-start(f32[2048]{0:T(1024)} %param.32) | copy-start | bytes 24580
  321.2 192.3 %all-to-all-start.4 = ((bf16[32,512,64]{1,2,0:T(8,128)(2,1)}), bf16[32,512,64]{1,2,0:T(8,128)(2,1)}, u32[]{:S(2)}, u32[]{:S(2)}) async-start(bf16[32,512,64]{1,2,0:T(8,128)(2,1)} %broadcast_in_dim.25), calls=%async_computation.4 | async-start | bytes 4194304 | tf_op jit(solution)/shard_map/all_to_all | solution.py:27
  509.6 2.8 copy-start.1
  564.2 8.9 %all-to-all-start.6 = ((f32[8,1,384]{2,1,0:T(1,128)}), f32[8,1,384]{2,1,0:T(1,128)S(1)}, u32[]{:S(2)}, u32[]{:S(2)}) async-start(f32[8,1,384]{2,1,0:T(1,128)} %broadcast_in_dim.26), calls=%async_computation.6 | async-start | bytes 24576 | tf_op jit(solution)/shard_map/all_to_all | solution.py:27
Sparse Core Ops, SparseCore 0:
  9.4 208.2 all-gather.2
  301.8 207.7 all-gather.4
where the time goes:
time: 582 us; the launch traced here: 581 us
  waiting for transfers between devices  383 us (66%)
  blocking collectives  93.2 us (16%)
  starting transfers between devices  42.3 us (7%)
  local copies, waits for them, and re-layouts  21.7 us (4%)
  between operations  14.1 us (2%)
  other arithmetic  13.3 us (2%)
  matrix products  12.9 us (2%)
    all_gather x2, waiting for transfers between devices, in_one_piece(): lax.all_gather(both, axis, axis=dim, tiled=True)  339 us
    all_to_all x2, blocking collectives, sent_and_summed(): lax.all_to_all(cut_along(shard, dim, peers), axis, 0, 0, tiled=True)  93.2 us
    all_to_all x5, waiting for transfers between devices, from_everyone(): return lax.all_to_all(copies, axis, split_axis=0, concat_axis=0, tiled=True)  44.5 us
    all_to_all x5, starting transfers between devices, from_everyone(): return lax.all_to_all(copies, axis, split_axis=0, concat_axis=0, tiled=True)  42.3 us
  transfers between devices with their start and end apart: 7, of which 5 were waited for; matrix products, arithmetic and copies ran while one was open for 6% of the time, Pallas kernels for 0%

commit v1 on v0

v1 whole, which is shorter than its diff:
```python
import functools

import jax
import jax.numpy as jnp
from jax import lax
from jax.experimental import pallas as pl
from jax.experimental.pallas import tpu as pltpu
from jax.sharding import PartitionSpec as P

EPS = 1e-06
GATE_POWER = 8.0
MESH = pl.DeviceIdType.MESH
NY, NZ, NX, NC = 4, 8, 4, 2
ZRING = 16
F32, BF16 = jnp.float32, jnp.bfloat16

FIRST_Y = (True, False, True, False, False, True)
LAGS = (0, 0, 1, 1, 2, 3)
LOG = []


class Net:
    def __init__(self, ssem, rsem):
        self.ssem, self.rsem = ssem, rsem
        self.count = 0
        self.started = []

    def send(self, src, dst, device, link):
        i = self.count
        self.count += 1
        copy = pltpu.make_async_remote_copy(
            src_ref=src, dst_ref=dst, send_sem=self.ssem.at[i], recv_sem=self.rsem.at[i],
            device_id=device, device_id_type=MESH,
        )
        copy.start()
        n = 1
        for s in src.shape:
            n *= s
        LOG.append(("start", link, n * src.dtype.itemsize, i))
        self.started.append(copy)
        copy.number = i
        return copy

    def arrived(self, copy):
        LOG.append(("wait", copy.number))
        copy.wait_recv()

    def drain(self):
        for copy in self.started:
            copy.wait_send()


def work(us):
    LOG.append(("work", us))


def sigmoid(v):
    return 1.0 / (1.0 + jnp.exp(-v))


def gelu(v):
    return 0.5 * v * (1.0 + jnp.tanh(0.7978845608028654 * (v + 0.044715 * (v * v * v))))


def softplus(v):
    t = jnp.exp(-jnp.abs(v))
    u = 1.0 + t
    small = u == 1.0
    log1p = jnp.where(small, t, jnp.log(u) * (t / jnp.where(small, 1.0, u - 1.0)))
    return jnp.maximum(v, 0.0) + log1p


def one_minus_exp(v):
    term = 1.0 + v * (1.0 / 9.0)
    for k in (8, 7, 6, 5, 4, 3, 2):
        term = 1.0 + v * (1.0 / k) * term
    return jnp.where(v > -0.5, -v * term, 1.0 - jnp.exp(v))


def nn(a, b):
    return lax.dot_general(a, b, (((1,), (0,)), ((), ())), preferred_element_type=F32)


def nt(a, b):
    return lax.dot_general(a, b, (((1,), (1,)), ((), ())), preferred_element_type=F32)


def layer_kernel(
    stream, w_in, w_gate, w_out, w_fg, w_fv, w_down,
    rgm, igm, rate, rtaps, spike, gtaps, vtaps, gain_r, gain_f, gain_c,
    out,
    g_in, g_gate, g_out, g_fg, g_fv, g_down,
    s_all, m_all, normed, pad_r, gate_src, mixed, pad_g, pad_v, hidden,
    own_sum, part_a, got_a, far_a, near_a, relay_a, fin_a,
    part_b, got_b, far_b, near_b, relay_b, fin_b,
    final, stats, ssem, rsem, lsem,
):
    rep, fs, tp = lax.axis_index("rep"), lax.axis_index("fs"), lax.axis_index("tp")
    zlo, y = fs // NY, fs % NY
    x, core = tp // NC, tp % NC
    z = rep * NZ + zlo
    zs = [(z + k) % ZRING for k in (1, ZRING - 1)]
    ys = [(y + k) % NY for k in (1, NY - 1)]
    xs = [(x + k) % NX for k in (1, NX - 1)]

    def at_z(zz):
        return {"rep": zz // NZ, "fs": (zz % NZ) * NY + y, "tp": tp}

    def at_y(yy):
        return {"rep": rep, "fs": zlo * NY + yy, "tp": tp}

    def at_x(xx, cc):
        return {"rep": rep, "fs": fs, "tp": xx * NC + cc}

    zup, zdn = at_z(zs[0]), at_z(zs[1])
    yup, ydn = at_y(ys[0]), at_y(ys[1])
    xup, xdn = at_x(xs[0], core), at_x(xs[1], core)
    pair = at_x(x, 1 - core)
    xfar = (x + 2) % NX

    shards = (w_in, w_gate, w_out, w_fg, w_fv, w_down)
    wholes = (g_in, g_gate, g_out, g_fg, g_fv, g_down)
    loads = [pltpu.make_async_copy(stream, s_all.at[tp], lsem.at[6])]
    for i in range(6):
        loads.append(pltpu.make_async_copy(shards[i], wholes[i].at[zlo, y], lsem.at[i]))
    for copy in loads:
        copy.start()

    others = [at_x(xx, cc) for xx in (xs[0], xs[1], xfar) for cc in (core, 1 - core)] + [pair]
    barrier = pltpu.get_barrier_semaphore()
    friends = [zup, zdn, yup, ydn] + others
    for friend in friends:
        pl.semaphore_signal(barrier, inc=1, device_id=friend, device_id_type=MESH)
    pl.semaphore_wait(barrier, len(friends))
    work(2.5)
    for copy in loads:
        copy.wait()

    net = Net(ssem, rsem)
    flight = [{} for _ in range(6)]

    def zslot(k):
        return (zlo + k + NZ) % NZ

    def yslot(k):
        return (y + k + NY) % NY

    def both(i, key, up_src, dn_src, up, dn, links):
        flight[i][key] = (net.send(up_src, up_src, up, links[0]), net.send(dn_src, dn_src, dn, links[1]))

    def landed(i, key):
        for copy in flight[i][key]:
            net.arrived(copy)

    def step(i, s):
        g = wholes[i]
        first_y = FIRST_Y[i]
        zl, yl = ("z+", "z-"), ("y+", "y-")
        if first_y:
            if s == 0:
                own = g.at[zlo, y]
                both(i, 0, own, own, yup, ydn, yl)
            elif s == 1:
                landed(i, 0)
                half = g.shape[2] // 2
                both(i, 1, g.at[zlo, yslot(-1), pl.ds(0, half)], g.at[zlo, yslot(1), pl.ds(half, half)], yup, ydn, yl)
            elif s == 2:
                landed(i, 1)
                both(i, 2, g.at[zlo], g.at[zlo], zup, zdn, zl)
            elif s in (3, 4):
                landed(i, s - 1)
                both(i, s, g.at[zslot(2 - s)], g.at[zslot(s - 2)], zup, zdn, zl)
            elif s == 5:
                landed(i, 4)
                both(i, 5, g.at[zslot(-3), pl.ds(0, 2)], g.at[zslot(3), pl.ds(2, 2)], zup, zdn, zl)
            else:
                landed(i, 5)
        else:
            if s == 0:
                own = g.at[zlo, y]
                both(i, 0, own, own, zup, zdn, zl)
            elif s in (1, 2):
                landed(i, s - 1)
                both(i, s, g.at[zslot(-s), y], g.at[zslot(s), y], zup, zdn, zl)
            elif s == 3:
                landed(i, 2)
                half = g.shape[2] // 2
                both(i, 3, g.at[zslot(-3), y, pl.ds(0, half)], g.at[zslot(3), y, pl.ds(half, half)], zup, zdn, zl)
            elif s == 4:
                landed(i, 3)
                both(i, 4, g.at[:, y], g.at[:, y], yup, ydn, yl)
            elif s == 5:
                landed(i, 4)
                both(i, 5, g.at[pl.ds(0, 4), yslot(-1)], g.at[pl.ds(4, 4), yslot(1)], yup, ydn, yl)
            else:
                landed(i, 5)

    queue = sorted((LAGS[i] + s, i, s) for i in range(6) for s in range(7))
    done = [0]

    def pump(upto):
        while done[0] < len(queue) and queue[done[0]][0] <= upto:
            _, i, s = queue[done[0]]
            step(i, s)
            done[0] += 1

    rows = stream.shape[0]
    cols = stream.shape[1]
    half_rows = rows // 2
    top, low = pl.ds(0, half_rows), pl.ds(half_rows, half_rows)

    def share_start(buf):
        own = buf.at[tp]
        up = net.send(own, own, xup, "x+")
        dn = net.send(own, own, xdn, "x-")
        return [up, dn, net.send(own, own, pair, "d")]

    def share_relay(buf, got):
        pairs = [got[2]]
        left, right = xs[1] * NC + core, xs[0] * NC + core
        net.arrived(got[0])
        up = net.send(buf.at[left, top], buf.at[left, top], xup, "x+")
        pairs.append(net.send(buf.at[left], buf.at[left], pair, "d"))
        net.arrived(got[1])
        dn = net.send(buf.at[right, low], buf.at[right, low], xdn, "x-")
        pairs.append(net.send(buf.at[right], buf.at[right], pair, "d"))
        return [up, dn], pairs

    def share_finish(buf, got, pairs):
        for copy in got:
            net.arrived(copy)
        far = xfar * NC + core
        pairs.append(net.send(buf.at[far], buf.at[far], pair, "d"))
        for copy in pairs:
            net.arrived(copy)

    def norm_into(buf, gain):
        chunk = 32

        def body(r, _):
            at = pl.multiple_of(r * chunk, chunk)
            total = jnp.zeros((chunk, cols), F32)
            for b in range(NX * NC):
                v = buf[b, pl.ds(at, chunk), :].astype(F32)
                total = total + v * v
            inverse = lax.rsqrt(jnp.sum(total, axis=1, keepdims=True) * (1.0 / (cols * NX * NC)) + EPS)
            for b in range(NX * NC):
                v = buf[b, pl.ds(at, chunk), :].astype(F32)
                normed[pl.ds(at, chunk), b * cols : (b + 1) * cols] = (
                    v * inverse * gain[:, b * cols : (b + 1) * cols]
                ).astype(BF16)
            return 0

        lax.fori_loop(0, rows // chunk, body, 0)
        work(1.5)

    def weight(i):
        g = wholes[i]
        return g[...].reshape(NZ * NY * g.shape[2], g.shape[3])

    def scatter_sum(lhs, i, part, got, far, near, relay, fin, between):
        g = wholes[i]
        a = lhs[...]
        to_pair = []
        for o in (2, 1, 3, 0):
            xd = (x + o) % NX
            theirs = g[xd * NC + (1 - core)].reshape(NY * g.shape[2], g.shape[3])
            part[o] = nt(a, theirs).astype(BF16)
            to_pair.append((o, net.send(part.at[o], got.at[o], pair, "d")))
            mine = g[xd * NC + core].reshape(NY * g.shape[2], g.shape[3])
            own_sum[o] = nt(a, mine)
            work(0.7)
        pairs = dict(to_pair)
        net.arrived(pairs[2])
        far[...] = (own_sum[2] + got[2].astype(F32)).astype(BF16)
        work(0.2)
        up = net.send(far.at[top], relay.at[0], xup, "x+")
        dn = net.send(far.at[low], relay.at[1], xdn, "x-")
        net.arrived(pairs[1])
        near[0, low, :] = (own_sum[1, low, :] + got[1, low, :].astype(F32)).astype(BF16)
        up1 = net.send(near.at[0, low], fin.at[0, low], xup, "x+")
        net.arrived(pairs[3])
        near[1, top, :] = (own_sum[3, top, :] + got[3, top, :].astype(F32)).astype(BF16)
        dn1 = net.send(near.at[1, top], fin.at[1, top], xdn, "x-")
        work(0.2)
        between()
        net.arrived(up)
        near[0, top, :] = (own_sum[1, top, :] + got[1, top, :].astype(F32) + relay[0].astype(F32)).astype(BF16)
        up2 = net.send(near.at[0, top], fin.at[0, top], xup, "x+")
        net.arrived(dn)
        near[1, low, :] = (own_sum[3, low, :] + got[3, low, :].astype(F32) + relay[1].astype(F32)).astype(BF16)
        dn2 = net.send(near.at[1, low], fin.at[1, low], xdn, "x-")
        work(0.2)
        net.arrived(pairs[0])
        for copy in (up1, dn1, up2, dn2):
            net.arrived(copy)
        work(0.3)
        return own_sum[0] + got[0].astype(F32) + fin[0].astype(F32) + fin[1].astype(F32)

    got = share_start(s_all)
    pump(0)
    got, pairs = share_relay(s_all, got)
    pump(1)
    share_finish(s_all, got, pairs)
    pump(2)
    norm_into(s_all, gain_r)
    pump(6)

    rec_in = nn(normed[...], weight(0)).astype(BF16)
    pad_r[0:8, :] = jnp.zeros((8, cols), F32)
    pad_r[8:, :] = rec_in.astype(F32)
    gate_src[...] = nn(normed[...], weight(1)).astype(BF16)
    work(2.0)
    pump(7)

    heads, block = rgm.shape[0], rgm.shape[1]
    base = GATE_POWER * softplus(-rate[...])
    carry = jnp.zeros((1, cols), F32)
    piece = 64
    for r in range(rows // piece):
        lo = r * piece
        conv = rtaps[0:1, :] * pad_r[8 - 3 + lo : 8 - 3 + lo + piece, :]
        for k in range(1, 4):
            conv = conv + rtaps[k : k + 1, :] * pad_r[8 - 3 + k + lo : 8 - 3 + k + lo + piece, :]
        conv = conv.astype(BF16)
        reset, admit, jumps = [], [], []
        for h in range(heads):
            blk = conv[:, h * block : (h + 1) * block]
            reset.append(nn(blk, rgm[h]))
            admit.append(nn(blk, igm[h]))
            jumps.append(jnp.broadcast_to(spike[lo : lo + piece, h : h + 1], (piece, block)))
        reset = sigmoid(jnp.concatenate(reset, axis=1))
        admit = sigmoid(jnp.concatenate(admit, axis=1))
        log_decay = -reset * base + jnp.concatenate(jumps, axis=1)
        a = jnp.exp(log_decay)
        b = jnp.sqrt(one_minus_exp(2.0 * log_decay)) * admit * conv.astype(F32)
        row = lax.broadcasted_iota(jnp.int32, (piece, cols), 0)
        d = 1
        while d < piece:
            if d < 8:
                keep = row >= d
                pa = jnp.where(keep, pltpu.roll(a, d, 0), 1.0)
                pb = jnp.where(keep, pltpu.roll(b, d, 0), 0.0)
            else:
                pa = jnp.concatenate([jnp.ones((d, cols), F32), a[: piece - d]], axis=0)
                pb = jnp.concatenate([jnp.zeros((d, cols), F32), b[: piece - d]], axis=0)
            b = a * pb + b
            a = a * pa
            d *= 2
        states = a * carry + b
        carry = states[piece - 1 : piece, :]
        mixed[lo : lo + piece, :] = (states * gelu(gate_src[lo : lo + piece, :].astype(F32))).astype(BF16)
    work(4.0)
    pump(8)

    branch = scatter_sum(
        mixed, 2, part_a, got_a, far_a, near_a, relay_a, fin_a, lambda: pump(8)
    ).astype(BF16)
    m_all[tp] = (s_all[tp].astype(F32) + branch.astype(F32)).astype(BF16)

    got = share_start(m_all)
    pump(8)
    got, pairs = share_relay(m_all, got)
    pump(8)
    share_finish(m_all, got, pairs)
    norm_into(m_all, gain_f)
    pump(9)

    wide = g_fg.shape[3]
    for pad, i in ((pad_g, 3), (pad_v, 4)):
        pad[0:8, :] = jnp.zeros((8, wide), F32)
        for j in range(0, wide, 256):
            w = wholes[i][:, :, :, j : j + 256].reshape(NZ * NY * wholes[i].shape[2], 256)
            pad[8:, j : j + 256] = nn(normed[...], w).astype(BF16).astype(F32)
        work(2.0)
    for r in range(rows // piece):
        lo = r * piece
        gate = gtaps[0:1, :] * pad_g[6 + lo : 6 + lo + piece, :]
        value = vtaps[0:1, :] * pad_v[6 + lo : 6 + lo + piece, :]
        for k in range(1, 3):
            gate = gate + gtaps[k : k + 1, :] * pad_g[6 + k + lo : 6 + k + lo + piece, :]
            value = value + vtaps[k : k + 1, :] * pad_v[6 + k + lo : 6 + k + lo + piece, :]
        hidden[lo : lo + piece, :] = (gelu(gate) * value).astype(BF16)
    work(1.5)
    pump(99)

    branch = scatter_sum(
        hidden, 5, part_b, got_b, far_b, near_b, relay_b, fin_b, lambda: None
    ).astype(BF16)
    last = m_all[tp].astype(F32) + branch.astype(F32)
    final[...] = last
    squares = last * last
    lanes = squares[:, 0:128] + squares[:, 128:256]
    sums = jnp.sum(lanes.T, axis=0, keepdims=True)
    stats[tp] = jnp.broadcast_to(sums, (8, rows))
    sent = [net.send(stats.at[tp], stats.at[tp], device, "s") for device in others]
    for copy in sent:
        net.arrived(copy)
    total = stats[0]
    for k in range(1, NX * NC):
        total = total + stats[k]
    inverse = lax.rsqrt(total * (1.0 / (cols * NX * NC)) + EPS).T[:, 0:1]
    gain = gain_c[:, pl.ds(pl.multiple_of(tp * cols, cols), cols)]
    out[...] = (final[...] * inverse * gain).astype(BF16)
    net.drain()


def shards(
    stream, recurrence_input_weight, output_gate_weight, recurrence_gate_matrix, input_gate_matrix,
    channel_decay_rate, recurrence_taps, spike_log_decay, recurrence_output_weight, feedforward_gate_upward,
    feedforward_value_upward, feedforward_gate_taps, feedforward_value_taps, feedforward_down_weight,
    recurrence_norm_gain, feedforward_norm_gain, closing_norm_gain,
):
    rows, cols = stream.shape
    tps = NX * NC
    weights = (
        recurrence_input_weight, output_gate_weight, recurrence_output_weight.T,
        feedforward_gate_upward, feedforward_value_upward, feedforward_down_weight.T,
    )
    wide = feedforward_gate_upward.shape[1]
    hbm = pl.BlockSpec(memory_space=pltpu.MemorySpace.HBM)
    vmem = pl.BlockSpec(memory_space=pltpu.VMEM)
    scatter = [
        pltpu.VMEM((NX, rows, cols), BF16),
        pltpu.VMEM((NX, rows, cols), BF16),
        pltpu.VMEM((rows, cols), BF16),
        pltpu.VMEM((2, rows, cols), BF16),
        pltpu.VMEM((2, rows // 2, cols), BF16),
        pltpu.VMEM((2, rows, cols), BF16),
    ]
    return pl.pallas_call(
        layer_kernel,
        out_shape=jax.ShapeDtypeStruct((rows, cols), BF16),
        in_specs=[hbm] * 7 + [vmem] * 10,
        out_specs=vmem,
        scratch_shapes=[pltpu.VMEM((NZ, NY, *w.shape), BF16) for w in weights]
        + [
            pltpu.VMEM((tps, rows, cols), BF16),
            pltpu.VMEM((tps, rows, cols), BF16),
            pltpu.VMEM((rows, tps * cols), BF16),
            pltpu.VMEM((rows + 8, cols), F32),
            pltpu.VMEM((rows, cols), BF16),
            pltpu.VMEM((rows, cols), BF16),
            pltpu.VMEM((rows + 8, wide), F32),
            pltpu.VMEM((rows + 8, wide), F32),
            pltpu.VMEM((rows, wide), BF16),
            pltpu.VMEM((NX, rows, cols), F32),
        ]
        + scatter + scatter
        + [
            pltpu.VMEM((rows, cols), F32),
            pltpu.VMEM((tps, 8, rows), F32),
            pltpu.SemaphoreType.DMA((160,)),
            pltpu.SemaphoreType.DMA((160,)),
            pltpu.SemaphoreType.DMA((7,)),
        ],
        compiler_params=pltpu.CompilerParams(
            collective_id=0, has_side_effects=True, vmem_limit_bytes=60 * 1024 * 1024
        ),
        name="layer",
    )(
        stream, *weights,
        recurrence_gate_matrix, input_gate_matrix, channel_decay_rate.reshape(1, -1), recurrence_taps,
        spike_log_decay, feedforward_gate_taps, feedforward_value_taps,
        recurrence_norm_gain.reshape(1, -1), feedforward_norm_gain.reshape(1, -1), closing_norm_gain.reshape(1, -1),
    )


def solution(mesh):
    in_specs = (
        P(("rep", "fs"), "tp"), P("fs", "tp"), P("fs", "tp"), P("tp", None, None), P("tp", None, None), P("tp"),
        P(None, "tp"), P(("rep", "fs"), "tp"), P("tp", "fs"), P("fs", "tp"), P("fs", "tp"), P(None, "tp"),
        P(None, "tp"), P("tp", "fs"), P(), P(), P(),
    )
    return jax.shard_map(
        shards, mesh=mesh, in_specs=in_specs, out_specs=P(("rep", "fs"), "tp"), check_vma=False
    )
```

time: 582 us -> 139 us (0.24)
  waiting for transfers between devices: 383 us -> 0 us
  Pallas kernels: 0 us -> 136 us
  blocking collectives: 93.2 us -> 0 us
  starting transfers between devices: 42.3 us -> 0 us
  local copies, waits for them, and re-layouts: 21.7 us -> 3.12 us
  between operations: 14.1 us -> 0.01 us
  other arithmetic: 13.3 us -> 0 us
  matrix products: 12.9 us -> 0 us
    all_gather x2 -> x0, waiting for transfers between devices: 339 us -> none  [in_one_piece(): lax.all_gather(both, axis, axis=dim, tiled=True)]
    pallas_call x0 -> x1, Pallas kernels: none -> 136 us  [shards(): pl.pallas_call(layer_kernel, out_shape=jax.ShapeDtypeStruct((rows, cols),...]
    all_to_all x2 -> x0, blocking collectives: 93.2 us -> none  [sent_and_summed(): lax.all_to_all(cut_along(shard, dim, peers), axis, 0, 0, tiled=True)]
    all_to_all x5 -> x0, waiting for transfers between devices: 44.5 us -> none  [from_everyone(): return lax.all_to_all(copies, axis, split_axis=0, concat_axis=0, tiled=True)]
    all_to_all x5 -> x0, starting transfers between devices: 42.3 us -> none  [from_everyone(): return lax.all_to_all(copies, axis, split_axis=0, concat_axis=0, tiled=True)]
    dot_general x7 -> x0, matrix products: 12.9 us -> none  [the longest x2 6.64 us: project_with(): jnp.dot(left_rows, weight_piece, preferred_element_type=jnp.float32)]
    slice x52 -> x0, local copies, waits for them, and re-layouts: 11.4 us -> none  [the longest x49 11.4 us: shards(): states = lax.associative_scan(chain_step, (decay_rate, inflow), axis=0)[1]]
    broadcast_in_dim x5 -> x0, local copies, waits for them, and re-layouts: 5.91 us -> none  [from_everyone(): copies = jnp.broadcast_to(shard, (lax.axis_size(axis), *shard.shape))]
  transfers between devices with their start and end apart: 7 -> 0, of which waited for: 5 -> 0; matrix products, arithmetic and copies ran while one was open for 6% -> 0% of each run, Pallas kernels for 0% -> 0%
where the time goes in v1:
time: 139 us
  Pallas kernels  136 us (98%)
  local copies, waits for them, and re-layouts  3.12 us (2%)
    pallas_call x1, Pallas kernels, shards(): pl.pallas_call(layer_kernel, out_shape=jax.ShapeDtypeStruct((rows, cols),...  136 us
    unnamed x4, local copies, waits for them, and re-layouts  3.12 us

profile of v1, /device:TPU:1, one launch (start us, length us, event | category | flops | bytes accessed | tf_op | source)
XLA Modules:
  0.0 138.9 jit_solution(17796752733731243880)
XLA Ops:
  0.0 0.0 copy-start
  0.0 0.7 copy-done
  0.7 0.8 copy.18.spike
  1.5 135.8 %layer.1 = bf16[384,256]{1,0:T(8,128)(2,1)} custom-call(bf16[384,256]{1,0:T(8,128)(2,1)} %stream.1, bf16[64,256]{1,0:T(8,128)(2,1)} %w_in.1, bf16[64,256]{1,0:T(8,128)(2,1)} %w_gate.1, bf16[64,256]{1,0:T(8,128)(2,1)} %bitcast.7, bf16[64,512]{1,0:T(8,128)(2,1)} %w_fg.1, bf16[64,512]{1,0:T(8,128)(2,1)} %w_fv.1, bf16[64,512]{1,0:T(8,128)(2,1)} %bitcast.6, ...), custom_call_target="tpu_custom_call" | custom-call | tf_op jit(solution)/shard_map/layer/pallas_call | solution.py:431
  137.3 1.6 %copy.20 = bf16[384,256]{1,0:T(8,128)(2,1)} copy(bf16[384,256]{1,0:T(8,128)(2,1)} %layer.1) | data formatting | bytes 393216
Async XLA Ops:
  0.0 0.7 copy-start

commit v2 on v1

v2 whole, which is shorter than its diff:
```python
import functools

import jax
import jax.numpy as jnp
from jax import lax
from jax.experimental import pallas as pl
from jax.experimental.pallas import tpu as pltpu
from jax.sharding import PartitionSpec as P

EPS = 1e-06
GATE_POWER = 8.0
MESH = pl.DeviceIdType.MESH
NY, NZ, NX, NC = 4, 8, 4, 2
ZRING = 16
F32, BF16 = jnp.float32, jnp.bfloat16

FIRST_Y = (True, False, True, False, False, True)
FINE = (True, True, False, False, False, False)
CHUNKS = 2
LOG = []
ORDER = (
    "w1.0", "w1.y1", "w4.0", "w1.y0", "s0", "w1.y2", "w0.00", "w2.0", "w3.0", "w5.0", "w1.1", "w1.r1", "w1.y4", "w4.1",
    "w1.r2", "w1.r0", "w1.y3", "w0.01", "w2.1", "s1", "w3.1", "w5.1", "w0.a", "w1.2", "w1.r4", "w1.y5", "w4.2", "w1.r3",
    "w1.y6", "w2.2", "s2", "w0.b", "w1.r5", "s3", "N0", "N1", "w1.3", "w4.3", "w1.r6", "w0.10", "w0.30", "w0.20",
    "w1.y7", "w3.2", "w4.4", "w0.11", "w0.31", "w0.21", "w2.3", "w0.32", "w0.22", "w0.12", "w0.02", "w2.4", "w1.r7", "w0.13",
    "w0.23", "w0.03", "w0.33", "w3.3", "w4.5", "W1", "P1", "w2.5", "w5.2", "W0", "P0", "R0", "R1", "W2",
    "R2", "w3.4", "a0m2", "a0m3", "R3", "R4", "a0f", "a0m1", "R5", "a1m2", "a0n", "a1m1", "w5.3", "a1f",
    "a0m0", "a1m0", "a0r", "W4", "a1m3", "a1n", "a1r", "a0e", "m00", "a1e", "m10", "w5.4", "w3.5", "m01",
    "m11", "m02", "m03", "M0", "m12", "u041", "u040", "m13", "w5.5", "M1", "W3", "u030", "u031", "H0",
    "H1", "u140", "H2", "u131", "u141", "W5", "b0m2", "b0m1", "b0m3", "b0f", "u130", "b0n", "H3", "H4",
    "H5", "b1m2", "b1m0", "b1m1", "b1f", "b1m3", "b0r", "b0m0", "b1n", "b1r", "b0e", "b1e", "F0", "F1",
)


class Net:
    def __init__(self, ssem, rsem):
        self.ssem, self.rsem = ssem, rsem
        self.copies = {}
        self.taken = set()

    def send(self, key, src, dst, device, link):
        i = len(self.copies)
        copy = pltpu.make_async_remote_copy(
            src_ref=src, dst_ref=dst, send_sem=self.ssem.at[i], recv_sem=self.rsem.at[i],
            device_id=device, device_id_type=MESH,
        )
        copy.start()
        n = 1
        for s in src.shape:
            n *= s
        LOG.append(("start", link, n * src.dtype.itemsize, key))
        self.copies[key] = copy

    def take(self, *keys):
        for key in keys:
            if key not in self.taken:
                self.taken.add(key)
                LOG.append(("wait", key))
                with scope("wait_" + str(key)):
                    self.copies[key].wait_recv()

    def drain(self):
        for copy in self.copies.values():
            copy.wait_send()


def scope(name):
    return jax.named_scope(name)


def work(us):
    LOG.append(("work", us))


def sigmoid(v):
    return 1.0 / (1.0 + jnp.exp(-v))


def gelu(v):
    return 0.5 * v * (1.0 + jnp.tanh(0.7978845608028654 * (v + 0.044715 * (v * v * v))))


def softplus(v):
    t = jnp.exp(-jnp.abs(v))
    u = 1.0 + t
    small = u == 1.0
    log1p = jnp.where(small, t, jnp.log(u) * (t / jnp.where(small, 1.0, u - 1.0)))
    return jnp.maximum(v, 0.0) + log1p


def one_minus_exp(v):
    term = 1.0 + v * (1.0 / 9.0)
    for k in (8, 7, 6, 5, 4, 3, 2):
        term = 1.0 + v * (1.0 / k) * term
    return jnp.where(v > -0.5, -v * term, 1.0 - jnp.exp(v))


def nn(a, b):
    return lax.dot_general(a, b, (((1,), (0,)), ((), ())), preferred_element_type=F32)


def nt(a, b):
    return lax.dot_general(a, b, (((1,), (1,)), ((), ())), preferred_element_type=F32)


def layer_kernel(
    stream, w_in, w_gate, w_out, w_fg, w_fv, w_down,
    rgm, igm, rate, rtaps, spike, gtaps, vtaps, gain_r, gain_f, gain_c,
    out,
    g_in, g_gate, g_out, g_fg, g_fv, g_down,
    s_all, m_all, normed, pad_r, gate_src, mixed, pad_g, pad_v, hidden, carry,
    own_a, part_a, got_a, far_a, near_a, relay_a, fin_a,
    own_b, part_b, got_b, far_b, near_b, relay_b, fin_b,
    final, stats, ssem, rsem, lsem,
):
    rep, fs, tp = lax.axis_index("rep"), lax.axis_index("fs"), lax.axis_index("tp")
    zlo, y = fs // NY, fs % NY
    x, core = tp // NC, tp % NC
    z = rep * NZ + zlo
    zs = [(z + k) % ZRING for k in (1, ZRING - 1)]
    ys = [(y + k) % NY for k in (1, NY - 1)]
    xs = [(x + k) % NX for k in (1, NX - 1)]

    def at_z(zz):
        return {"rep": zz // NZ, "fs": (zz % NZ) * NY + y, "tp": tp}

    def at_y(yy):
        return {"rep": rep, "fs": zlo * NY + yy, "tp": tp}

    def at_x(xx, cc):
        return {"rep": rep, "fs": fs, "tp": xx * NC + cc}

    zup, zdn = at_z(zs[0]), at_z(zs[1])
    yup, ydn = at_y(ys[0]), at_y(ys[1])
    xup, xdn = at_x(xs[0], core), at_x(xs[1], core)
    pair = at_x(x, 1 - core)
    xfar = (x + 2) % NX

    shards = (w_in, w_gate, w_out, w_fg, w_fv, w_down)
    wholes = (g_in, g_gate, g_out, g_fg, g_fv, g_down)
    loads = [pltpu.make_async_copy(stream, s_all.at[tp], lsem.at[6])]
    for i in range(6):
        loads.append(pltpu.make_async_copy(shards[i], wholes[i].at[zlo, y], lsem.at[i]))
    for copy in loads:
        copy.start()

    others = [at_x(xx, cc) for xx in (xs[0], xs[1], xfar) for cc in (core, 1 - core)] + [pair]
    with scope("barrier"):
        barrier = pltpu.get_barrier_semaphore()
        friends = [zup, zdn, yup, ydn] + others
        for friend in friends:
            pl.semaphore_signal(barrier, inc=1, device_id=friend, device_id_type=MESH)
        pl.semaphore_wait(barrier, len(friends))
    with scope("loads"):
        for copy in loads:
            copy.wait()

    net = Net(ssem, rsem)
    items = {}

    def item(name, deps, *args):
        def add(fn):
            items[name] = (tuple(deps), functools.partial(fn, *args))
            return fn
        return add

    def zslot(k):
        return (zlo + k + NZ) % NZ

    def yslot(k):
        return (y + k + NY) % NY

    def both(key, up_src, dn_src, line):
        up, dn = (zup, zdn) if line == "z" else (yup, ydn)
        net.send(key + "+", up_src, up_src, up, line + "+")
        net.send(key + "-", dn_src, dn_src, dn, line + "-")

    def landed(key):
        net.take(key + "+", key + "-")

    def coarse(i, g):
        n = f"w{i}."
        half = g.shape[2] // 2
        steps = []
        if FIRST_Y[i]:
            steps = [
                lambda: both(n + "0", g.at[zlo, y], g.at[zlo, y], "y"),
                lambda: both(n + "1", g.at[zlo, yslot(-1), pl.ds(0, half)], g.at[zlo, yslot(1), pl.ds(half, half)], "y"),
                lambda: both(n + "2", g.at[zlo], g.at[zlo], "z"),
                lambda: both(n + "3", g.at[zslot(-1)], g.at[zslot(1)], "z"),
                lambda: both(n + "4", g.at[zslot(-2)], g.at[zslot(2)], "z"),
                lambda: both(n + "5", g.at[zslot(-3), pl.ds(0, 2)], g.at[zslot(3), pl.ds(2, 2)], "z"),
            ]
        else:
            steps = [
                lambda: both(n + "0", g.at[zlo, y], g.at[zlo, y], "z"),
                lambda: both(n + "1", g.at[zslot(-1), y], g.at[zslot(1), y], "z"),
                lambda: both(n + "2", g.at[zslot(-2), y], g.at[zslot(2), y], "z"),
                lambda: both(n + "3", g.at[zslot(-3), y, pl.ds(0, half)], g.at[zslot(3), y, pl.ds(half, half)], "z"),
                lambda: both(n + "4", g.at[:, y], g.at[:, y], "y"),
                lambda: both(n + "5", g.at[pl.ds(0, 4), yslot(-1)], g.at[pl.ds(4, 4), yslot(1)], "y"),
            ]

        def run(s):
            if s > 0:
                landed(n + str(s - 1))
            steps[s]()

        for s in range(6):
            item(n + str(s), [n + str(s - 1)] if s else [], s)(run)
        item(f"W{i}", [n + "5"])(lambda: landed(n + "5"))

    def fine_y(i, g):
        n = f"w{i}."
        half = g.shape[2] // 2
        item(n + "a", [])(lambda: both(n + "a", g.at[zlo, y], g.at[zlo, y], "y"))

        def relay():
            landed(n + "a")
            both(n + "b", g.at[zlo, yslot(-1), pl.ds(0, half)], g.at[zlo, yslot(1), pl.ds(half, half)], "y")

        item(n + "b", [n + "a"])(relay)
        before = ([], [n + "a"], [n + "a"], [n + "b"])

        def hop(j, o, k):
            if k == 0:
                if j == 1:
                    net.take(n + "a+")
                elif j == 2:
                    net.take(n + "a-")
                elif j == 3:
                    landed(n + "b")
            else:
                landed(f"{n}{j}{k - 1}")
            yy = yslot(o)
            if k < 3:
                both(f"{n}{j}{k}", g.at[zslot(-k), yy], g.at[zslot(k), yy], "z")
            else:
                both(f"{n}{j}{k}", g.at[zslot(-3), yy, pl.ds(0, half)], g.at[zslot(3), yy, pl.ds(half, half)], "z")

        for j, o in enumerate((0, -1, 1, 2)):
            for k in range(4):
                item(f"{n}{j}{k}", [f"{n}{j}{k - 1}"] if k else before[j], j, o, k)(hop)

        def end():
            for j in range(4):
                landed(f"{n}{j}3")

        item(f"W{i}", [f"{n}{j}3" for j in range(4)] + [n + "b"])(end)

    def fine_z(i, g):
        n = f"w{i}."
        half = g.shape[2] // 2

        def hop(k):
            if k:
                landed(f"{n}{k - 1}")
            if k < 3:
                both(f"{n}{k}", g.at[zslot(-k), y], g.at[zslot(k), y], "z")
            else:
                both(f"{n}{k}", g.at[zslot(-3), y, pl.ds(0, half)], g.at[zslot(3), y, pl.ds(half, half)], "z")

        for k in range(4):
            item(f"{n}{k}", [f"{n}{k - 1}"] if k else [], k)(hop)

        def side(m, o):
            if o == 4:
                landed(f"{n}3")
            elif o < 0:
                net.take(f"{n}{-o - 1}+")
            elif o > 0:
                net.take(f"{n}{o - 1}-")
            both(f"{n}y{m}", g.at[zslot(o), y], g.at[zslot(o), y], "y")

        def relay(m, o):
            landed(f"{n}y{m}")
            both(f"{n}r{m}", g.at[zslot(o), yslot(-1), pl.ds(0, half)], g.at[zslot(o), yslot(1), pl.ds(half, half)], "y")

        ms = (0, -1, 1, -2, 2, -3, 3, 4)
        for m, o in enumerate(ms):
            item(f"{n}y{m}", [f"{n}{abs(o) - 1}"] if o else [], m, o)(side)
            item(f"{n}r{m}", [f"{n}y{m}"], m, o)(relay)

        def end():
            for m in range(8):
                landed(f"{n}r{m}")

        item(f"W{i}", [f"{n}r{m}" for m in range(8)])(end)

    for i in range(6):
        if FINE[i]:
            (fine_y if FIRST_Y[i] else fine_z)(i, wholes[i])
        else:
            coarse(i, wholes[i])

    rows, cols = stream.shape
    span = rows // CHUNKS
    half_rows = span // 2

    def share(n, buf, lo, size, deps):
        whole, top, low = pl.ds(lo, size), pl.ds(lo, size // 2), pl.ds(lo + size // 2, size // 2)
        left, right, far = xs[1] * NC + core, xs[0] * NC + core, xfar * NC + core

        def start():
            own = buf.at[tp, whole]
            net.send(n + "0+", own, own, xup, "x+")
            net.send(n + "0-", own, own, xdn, "x-")
            net.send(n + "p0", own, own, pair, "d")

        def relay():
            net.take(n + "0+")
            net.send(n + "1+", buf.at[left, top], buf.at[left, top], xup, "x+")
            net.take(n + "0-")
            net.send(n + "1-", buf.at[right, low], buf.at[right, low], xdn, "x-")
            net.send(n + "p1", buf.at[left, whole], buf.at[left, whole], pair, "d")
            net.send(n + "p2", buf.at[right, whole], buf.at[right, whole], pair, "d")

        def last():
            net.take(n + "1+", n + "1-")
            net.send(n + "p3", buf.at[far, whole], buf.at[far, whole], pair, "d")

        item(n + "0", deps)(start)
        item(n + "1", [n + "0"])(relay)
        item(n + "2", [n + "1"])(last)
        item(n + "3", [n + "2"])(lambda: net.take(n + "p0", n + "p1", n + "p2", n + "p3"))

    chunk = 32

    def norm_rows(buf, gain, lo, size):
        def body(r, _):
            at = pl.multiple_of(lo + r * chunk, chunk)
            total = jnp.zeros((chunk, cols), F32)
            for b in range(NX * NC):
                v = buf[b, pl.ds(at, chunk), :].astype(F32)
                total = total + v * v
            inverse = lax.rsqrt(jnp.sum(total, axis=1, keepdims=True) * (1.0 / (cols * NX * NC)) + EPS)
            for b in range(NX * NC):
                v = buf[b, pl.ds(at, chunk), :].astype(F32)
                normed[pl.ds(at, chunk), b * cols : (b + 1) * cols] = (
                    v * inverse * gain[:, b * cols : (b + 1) * cols]
                ).astype(BF16)
            return 0

        lax.fori_loop(0, size // chunk, body, 0)
        work(1.5 * size / 384)

    def scatter(n, t, lhs, i, own, part, got, far, near, relay, fin, deps, finish):
        g = wholes[i]
        lo = t * span
        top, low = slice(0, half_rows), slice(half_rows, span)

        def mm(o):
            a = lhs[lo : lo + span, :]
            xd = (x + o) % NX
            theirs = g[xd * NC + (1 - core)].reshape(NY * g.shape[2], g.shape[3])
            part[t, o] = nt(a, theirs).astype(BF16)
            net.send(f"{n}d{o}", part.at[t, o], got.at[t, o], pair, "d")
            mine = g[xd * NC + core].reshape(NY * g.shape[2], g.shape[3])
            own[t, o] = nt(a, mine)
            work(0.4)

        def out_far():
            net.take(n + "d2")
            far[t] = (own[t, 2] + got[t, 2].astype(F32)).astype(BF16)
            work(0.1)
            net.send(n + "f+", far.at[t, pl.ds(0, half_rows)], relay.at[t, 0], xup, "x+")
            net.send(n + "f-", far.at[t, pl.ds(half_rows, half_rows)], relay.at[t, 1], xdn, "x-")

        def out_near():
            net.take(n + "d1", n + "d3")
            near[t, 0, low, :] = (own[t, 1, low, :] + got[t, 1, low, :].astype(F32)).astype(BF16)
            near[t, 1, top, :] = (own[t, 3, top, :] + got[t, 3, top, :].astype(F32)).astype(BF16)
            work(0.1)
            at = pl.ds(half_rows, half_rows)
            net.send(n + "n+", near.at[t, 0, at], fin.at[t, 0, at], xup, "x+")
            at = pl.ds(0, half_rows)
            net.send(n + "n-", near.at[t, 1, at], fin.at[t, 1, at], xdn, "x-")

        def out_relay():
            net.take(n + "f+", n + "f-")
            near[t, 0, top, :] = (own[t, 1, top, :] + got[t, 1, top, :].astype(F32) + relay[t, 0].astype(F32)).astype(BF16)
            near[t, 1, low, :] = (own[t, 3, low, :] + got[t, 3, low, :].astype(F32) + relay[t, 1].astype(F32)).astype(BF16)
            work(0.1)
            at = pl.ds(0, half_rows)
            net.send(n + "r+", near.at[t, 0, at], fin.at[t, 0, at], xup, "x+")
            at = pl.ds(half_rows, half_rows)
            net.send(n + "r-", near.at[t, 1, at], fin.at[t, 1, at], xdn, "x-")

        def end():
            net.take(n + "d0", n + "n+", n + "n-", n + "r+", n + "r-")
            finish(own[t, 0] + got[t, 0].astype(F32) + fin[t, 0].astype(F32) + fin[t, 1].astype(F32))

        for o in (2, 1, 3, 0):
            item(f"{n}m{o}", deps, o)(mm)
        item(n + "f", [n + "m2"])(out_far)
        item(n + "n", [n + "m1", n + "m3"])(out_near)
        item(n + "r", [n + "f", n + "n"])(out_relay)
        item(n + "e", [n + "r", n + "m0"])(end)

    share("s", s_all, 0, rows, [])
    for t in range(2):
        item(f"N{t}", ["s3"], s_all, gain_r, t * rows // 2, rows // 2)(norm_rows)

    def weight(i, j=0, n=0):
        g = wholes[i]
        return g[:, :, :, j : j + (n or g.shape[3])].reshape(NZ * NY * g.shape[2], n or g.shape[3])

    def project_in():
        rec_in = nn(normed[...], weight(0)).astype(BF16)
        pad_r[0:8, :] = jnp.zeros((8, cols), F32)
        pad_r[8:, :] = rec_in.astype(F32)
        work(1.0)

    def project_gate():
        gate_src[...] = nn(normed[...], weight(1)).astype(BF16)
        work(1.0)

    item("P0", ["N0", "N1", "W0"])(project_in)
    item("P1", ["N0", "N1", "W1"])(project_gate)

    heads, block = rgm.shape[0], rgm.shape[1]
    piece = 64

    def recur(r):
        base = GATE_POWER * softplus(-rate[...])
        lo = r * piece
        conv = rtaps[0:1, :] * pad_r[8 - 3 + lo : 8 - 3 + lo + piece, :]
        for k in range(1, 4):
            conv = conv + rtaps[k : k + 1, :] * pad_r[8 - 3 + k + lo : 8 - 3 + k + lo + piece, :]
        conv = conv.astype(BF16)
        reset, admit, jumps = [], [], []
        for h in range(heads):
            blk = conv[:, h * block : (h + 1) * block]
            reset.append(nn(blk, rgm[h]))
            admit.append(nn(blk, igm[h]))
            jumps.append(jnp.broadcast_to(spike[lo : lo + piece, h : h + 1], (piece, block)))
        reset = sigmoid(jnp.concatenate(reset, axis=1))
        admit = sigmoid(jnp.concatenate(admit, axis=1))
        log_decay = -reset * base + jnp.concatenate(jumps, axis=1)
        a = jnp.exp(log_decay)
        b = jnp.sqrt(one_minus_exp(2.0 * log_decay)) * admit * conv.astype(F32)
        row = lax.broadcasted_iota(jnp.int32, (piece, cols), 0)
        d = 1
        while d < piece:
            if d < 8:
                keep = row >= d
                pa = jnp.where(keep, pltpu.roll(a, d, 0), 1.0)
                pb = jnp.where(keep, pltpu.roll(b, d, 0), 0.0)
            else:
                pa = jnp.concatenate([jnp.ones((d, cols), F32), a[: piece - d]], axis=0)
                pb = jnp.concatenate([jnp.zeros((d, cols), F32), b[: piece - d]], axis=0)
            b = a * pb + b
            a = a * pa
            d *= 2
        states = b if r == 0 else a * carry[0:1, :] + b
        carry[0:1, :] = states[piece - 1 : piece, :]
        mixed[lo : lo + piece, :] = (states * gelu(gate_src[lo : lo + piece, :].astype(F32))).astype(BF16)
        work(0.7)

    per = span // piece
    for r in range(rows // piece):
        item(f"R{r}", ["P0", "P1"] + ([f"R{r - 1}"] if r else []), r)(recur)

    def to_middle(t, total):
        at = slice(t * span, (t + 1) * span)
        m_all[tp, at, :] = (s_all[tp, at, :].astype(F32) + total.astype(BF16).astype(F32)).astype(BF16)
        work(0.15)

    for t in range(CHUNKS):
        scatter(
            f"a{t}", t, mixed, 2, own_a, part_a, got_a, far_a, near_a, relay_a, fin_a,
            ["W2"] + [f"R{t * per + q}" for q in range(per)], functools.partial(to_middle, t),
        )
        share(f"m{t}", m_all, t * span, span, [f"a{t}e"])
        item(f"M{t}", [f"m{t}3", "P0", "P1"], m_all, gain_f, t * span, span)(norm_rows)

    wide = g_fg.shape[3]

    def up(t, i, pad, j):
        at = slice(t * span, (t + 1) * span)
        if t == 0:
            pad[0:8, j : j + 256] = jnp.zeros((8, 256), F32)
        pad[8 + t * span : 8 + (t + 1) * span, j : j + 256] = nn(normed[at, :], weight(i, j, 256)).astype(BF16).astype(F32)
        work(0.6)

    def mix(r):
        lo = r * piece
        gate = gtaps[0:1, :] * pad_g[6 + lo : 6 + lo + piece, :]
        value = vtaps[0:1, :] * pad_v[6 + lo : 6 + lo + piece, :]
        for k in range(1, 3):
            gate = gate + gtaps[k : k + 1, :] * pad_g[6 + k + lo : 6 + k + lo + piece, :]
            value = value + vtaps[k : k + 1, :] * pad_v[6 + k + lo : 6 + k + lo + piece, :]
        hidden[lo : lo + piece, :] = (gelu(gate) * value).astype(BF16)
        work(0.3)

    def to_final(t, total):
        at = slice(t * span, (t + 1) * span)
        last = m_all[tp, at, :].astype(F32) + total.astype(BF16).astype(F32)
        final[at, :] = last
        squares = last * last
        lanes = squares[:, 0:128] + squares[:, 128:256]
        sums = jnp.sum(lanes.T, axis=0, keepdims=True)
        stats[t, tp] = jnp.broadcast_to(sums, (8, span))
        work(0.5)
        for k, device in enumerate(others):
            net.send(f"q{t}{k}", stats.at[t, tp], stats.at[t, tp], device, "s")

    def finish(t):
        for k in range(len(others)):
            net.take(f"q{t}{k}")
        at = slice(t * span, (t + 1) * span)
        total = stats[t, 0]
        for k in range(1, NX * NC):
            total = total + stats[t, k]
        inverse = lax.rsqrt(total * (1.0 / (cols * NX * NC)) + EPS).T[:, 0:1]
        gain = gain_c[:, pl.ds(pl.multiple_of(tp * cols, cols), cols)]
        out[at, :] = (final[at, :] * inverse * gain).astype(BF16)
        work(0.4)

    for t in range(CHUNKS):
        ups = []
        for i, pad in ((3, pad_g), (4, pad_v)):
            for j in range(0, wide, 256):
                ups.append(f"u{t}{i}{j // 256}")
                item(ups[-1], [f"M{t}", f"W{i}"], t, i, pad, j)(up)
        for q in range(per):
            r = t * per + q
            item(f"H{r}", ups + ([f"H{r - 1}"] if r else []), r)(mix)
        scatter(
            f"b{t}", t, hidden, 5, own_b, part_b, got_b, far_b, near_b, relay_b, fin_b,
            ["W5"] + [f"H{t * per + q}" for q in range(per)], functools.partial(to_final, t),
        )
        item(f"F{t}", [f"b{t}e"])(functools.partial(finish, t))

    emitted = set()

    def emit(name):
        if name in emitted:
            return
        deps, fn = items[name]
        for dep in deps:
            emit(dep)
        LOG.append(("item", name, deps))
        with scope(name):
            fn()
        emitted.add(name)

    for name in ORDER:
        emit(name)
    for name in items:
        emit(name)
    LOG.append(("item", "drain", tuple(items)))
    with scope("drain"):
        net.drain()


def shards(
    stream, recurrence_input_weight, output_gate_weight, recurrence_gate_matrix, input_gate_matrix,
    channel_decay_rate, recurrence_taps, spike_log_decay, recurrence_output_weight, feedforward_gate_upward,
    feedforward_value_upward, feedforward_gate_taps, feedforward_value_taps, feedforward_down_weight,
    recurrence_norm_gain, feedforward_norm_gain, closing_norm_gain,
):
    rows, cols = stream.shape
    tps = NX * NC
    weights = (
        recurrence_input_weight, output_gate_weight, recurrence_output_weight.T,
        feedforward_gate_upward, feedforward_value_upward, feedforward_down_weight.T,
    )
    wide = feedforward_gate_upward.shape[1]
    hbm = pl.BlockSpec(memory_space=pltpu.MemorySpace.HBM)
    vmem = pl.BlockSpec(memory_space=pltpu.VMEM)
    span = rows // CHUNKS
    scatter = [
        pltpu.VMEM((CHUNKS, NX, span, cols), F32),
        pltpu.VMEM((CHUNKS, NX, span, cols), BF16),
        pltpu.VMEM((CHUNKS, NX, span, cols), BF16),
        pltpu.VMEM((CHUNKS, span, cols), BF16),
        pltpu.VMEM((CHUNKS, 2, span, cols), BF16),
        pltpu.VMEM((CHUNKS, 2, span // 2, cols), BF16),
        pltpu.VMEM((CHUNKS, 2, span, cols), BF16),
    ]
    return pl.pallas_call(
        layer_kernel,
        out_shape=jax.ShapeDtypeStruct((rows, cols), BF16),
        in_specs=[hbm] * 7 + [vmem] * 10,
        out_specs=vmem,
        scratch_shapes=[pltpu.VMEM((NZ, NY, *w.shape), BF16) for w in weights]
        + [
            pltpu.VMEM((tps, rows, cols), BF16),
            pltpu.VMEM((tps, rows, cols), BF16),
            pltpu.VMEM((rows, tps * cols), BF16),
            pltpu.VMEM((rows + 8, cols), F32),
            pltpu.VMEM((rows, cols), BF16),
            pltpu.VMEM((rows, cols), BF16),
            pltpu.VMEM((rows + 8, wide), F32),
            pltpu.VMEM((rows + 8, wide), F32),
            pltpu.VMEM((rows, wide), BF16),
            pltpu.VMEM((8, cols), F32),
        ]
        + scatter + scatter
        + [
            pltpu.VMEM((rows, cols), F32),
            pltpu.VMEM((CHUNKS, tps, 8, span), F32),
            pltpu.SemaphoreType.DMA((288,)),
            pltpu.SemaphoreType.DMA((288,)),
            pltpu.SemaphoreType.DMA((7,)),
        ],
        compiler_params=pltpu.CompilerParams(
            collective_id=0, has_side_effects=True, vmem_limit_bytes=60 * 1024 * 1024
        ),
        name="layer",
    )(
        stream, *weights,
        recurrence_gate_matrix, input_gate_matrix, channel_decay_rate.reshape(1, -1), recurrence_taps,
        spike_log_decay, feedforward_gate_taps, feedforward_value_taps,
        recurrence_norm_gain.reshape(1, -1), feedforward_norm_gain.reshape(1, -1), closing_norm_gain.reshape(1, -1),
    )


def solution(mesh):
    in_specs = (
        P(("rep", "fs"), "tp"), P("fs", "tp"), P("fs", "tp"), P("tp", None, None), P("tp", None, None), P("tp"),
        P(None, "tp"), P(("rep", "fs"), "tp"), P("tp", "fs"), P("fs", "tp"), P("fs", "tp"), P(None, "tp"),
        P(None, "tp"), P("tp", "fs"), P(), P(), P(),
    )
    return jax.shard_map(
        shards, mesh=mesh, in_specs=in_specs, out_specs=P(("rep", "fs"), "tp"), check_vma=False
    )
```

time: 139 us -> 112 us (0.81)
  Pallas kernels: 136 us -> 108 us
    pallas_call x1, Pallas kernels: 136 us -> 108 us  [shards(): pl.pallas_call(layer_kernel, out_shape=jax.ShapeDtypeStruct((rows, cols),...]
where the time goes in v2:
time: 112 us; the launch traced here: 111 us
  Pallas kernels  108 us (96%)
  local copies, waits for them, and re-layouts  3.12 us (3%)
    pallas_call x1, Pallas kernels, shards(): pl.pallas_call(layer_kernel, out_shape=jax.ShapeDtypeStruct((rows, cols),...  108 us
    unnamed x4, local copies, waits for them, and re-layouts  3.12 us

profile of v2, /device:TPU:1, one launch (start us, length us, event | category | flops | bytes accessed | tf_op | source)
XLA Modules:
  0.0 111.4 jit_solution(1574481279580446552)
XLA Ops:
  0.0 0.0 copy-start
  0.0 0.7 copy-done
  0.7 0.8 copy.18.spike
  1.5 108.2 %layer.1 = bf16[384,256]{1,0:T(8,128)(2,1)} custom-call(bf16[384,256]{1,0:T(8,128)(2,1)} %stream.1, bf16[64,256]{1,0:T(8,128)(2,1)} %w_in.1, bf16[64,256]{1,0:T(8,128)(2,1)} %w_gate.1, bf16[64,256]{1,0:T(8,128)(2,1)} %bitcast.7, bf16[64,512]{1,0:T(8,128)(2,1)} %w_fg.1, bf16[64,512]{1,0:T(8,128)(2,1)} %w_fv.1, bf16[64,512]{1,0:T(8,128)(2,1)} %bitcast.6, ...), custom_call_target="tpu_custom_call" | custom-call | tf_op jit(solution)/shard_map/layer/pallas_call | solution.py:582
  109.8 1.6 %copy.20 = bf16[384,256]{1,0:T(8,128)(2,1)} copy(bf16[384,256]{1,0:T(8,128)(2,1)} %layer.1) | data formatting | bytes 393216
Async XLA Ops:
  0.0 0.7 copy-start

commit v3 on v2

--- a/solution.py
+++ b/solution.py
@@ -15,53 +15,51 @@
 F32, BF16 = jnp.float32, jnp.bfloat16
 
 FIRST_Y = (True, False, True, False, False, True)
-FINE = (True, True, False, False, False, False)
+FINE = (True, True, True, True, True, True)
 CHUNKS = 2
+SEMS = 145
 LOG = []
 ORDER = (
-    "w1.0", "w1.y1", "w4.0", "w1.y0", "s0", "w1.y2", "w0.00", "w2.0", "w3.0", "w5.0", "w1.1", "w1.r1", "w1.y4", "w4.1",
-    "w1.r2", "w1.r0", "w1.y3", "w0.01", "w2.1", "s1", "w3.1", "w5.1", "w0.a", "w1.2", "w1.r4", "w1.y5", "w4.2", "w1.r3",
-    "w1.y6", "w2.2", "s2", "w0.b", "w1.r5", "s3", "N0", "N1", "w1.3", "w4.3", "w1.r6", "w0.10", "w0.30", "w0.20",
-    "w1.y7", "w3.2", "w4.4", "w0.11", "w0.31", "w0.21", "w2.3", "w0.32", "w0.22", "w0.12", "w0.02", "w2.4", "w1.r7", "w0.13",
-    "w0.23", "w0.03", "w0.33", "w3.3", "w4.5", "W1", "P1", "w2.5", "w5.2", "W0", "P0", "R0", "R1", "W2",
-    "R2", "w3.4", "a0m2", "a0m3", "R3", "R4", "a0f", "a0m1", "R5", "a1m2", "a0n", "a1m1", "w5.3", "a1f",
-    "a0m0", "a1m0", "a0r", "W4", "a1m3", "a1n", "a1r", "a0e", "m00", "a1e", "m10", "w5.4", "w3.5", "m01",
-    "m11", "m02", "m03", "M0", "m12", "u041", "u040", "m13", "w5.5", "M1", "W3", "u030", "u031", "H0",
-    "H1", "u140", "H2", "u131", "u141", "W5", "b0m2", "b0m1", "b0m3", "b0f", "u130", "b0n", "H3", "H4",
-    "H5", "b1m2", "b1m0", "b1m1", "b1f", "b1m3", "b0r", "b0m0", "b1n", "b1r", "b0e", "b1e", "F0", "F1",
+    42, 40, 0, 19, 120, 128, 129, 2, 23, 59, 63, 80, 101, 46, 1, 41, 20, 24, 27, 10, 65, 6,
+    121, 3, 86, 14, 47, 31, 21, 29, 54, 28, 7, 66, 11, 25, 122, 15, 64, 4, 32, 33, 123, 124,
+    22, 35, 50, 125, 8, 30, 84, 12, 16, 26, 43, 102, 55, 37, 51, 36, 34, 9, 67, 13, 5, 17,
+    48, 85, 44, 87, 56, 38, 88, 52, 81, 18, 126, 68, 49, 45, 39, 127, 53, 57, 130, 60, 89, 131,
+    132, 82, 92, 133, 134, 135, 115, 90, 58, 149, 151, 150, 71, 61, 152, 153, 136, 69, 138, 154, 83, 139,
+    94, 107, 137, 140, 103, 96, 155, 141, 62, 72, 111, 73, 142, 108, 70, 156, 157, 75, 116, 77, 104, 143,
+    144, 74, 112, 95, 97, 158, 109, 76, 98, 117, 145, 78, 105, 93, 159, 91, 113, 160, 161, 146, 110, 99,
+    118, 79, 178, 179, 106, 147, 148, 162, 114, 163, 100, 181, 164, 180, 165, 166, 167, 168, 119, 182, 183, 184,
+    169, 171, 173, 170, 185, 172, 174, 186, 175, 187, 176, 188, 177, 189,
 )
 
 
 class Net:
     def __init__(self, ssem, rsem):
         self.ssem, self.rsem = ssem, rsem
-        self.copies = {}
+        self.arrivals, self.departures = {}, {}
         self.taken = set()
 
-    def send(self, key, src, dst, device, link):
-        i = len(self.copies)
+    def send(self, key, leave, src, dst, device, link):
         copy = pltpu.make_async_remote_copy(
-            src_ref=src, dst_ref=dst, send_sem=self.ssem.at[i], recv_sem=self.rsem.at[i],
+            src_ref=src, dst_ref=dst,
+            send_sem=self.ssem.at[self.departures.setdefault(leave, len(self.departures))],
+            recv_sem=self.rsem.at[self.arrivals.setdefault(key, len(self.arrivals))],
             device_id=device, device_id_type=MESH,
         )
         copy.start()
         n = 1
-        for s in src.shape:
-            n *= s
+        for size in src.shape:
+            n *= size
         LOG.append(("start", link, n * src.dtype.itemsize, key))
-        self.copies[key] = copy
-
-    def take(self, *keys):
-        for key in keys:
-            if key not in self.taken:
-                self.taken.add(key)
-                LOG.append(("wait", key))
-                with scope("wait_" + str(key)):
-                    self.copies[key].wait_recv()
-
-    def drain(self):
-        for copy in self.copies.values():
-            copy.wait_send()
+
+    def take(self, key, ref):
+        LOG.append(("wait", key))
+        if key not in self.taken:
+            self.taken.add(key)
+            with scope("wait_" + key):
+                pltpu.make_async_copy(ref, ref, self.rsem.at[self.arrivals[key]]).wait()
+
+    def left(self, leave, ref):
+        pltpu.make_async_copy(ref, ref, self.ssem.at[self.departures.pop(leave)]).wait()
 
 
 def scope(name):
@@ -105,13 +103,15 @@
 
 def layer_kernel(
     stream, w_in, w_gate, w_out, w_fg, w_fv, w_down,
-    rgm, igm, rate, rtaps, spike, gtaps, vtaps, gain_r, gain_f, gain_c,
+    rgm_h, igm_h, rate_h, rtaps_h, spike_h, gtaps_h, vtaps_h, gain_r_h, gain_f_h, gain_c_h,
     out,
     g_in, g_gate, g_out, g_fg, g_fv, g_down,
     s_all, m_all, normed, pad_r, gate_src, mixed, pad_g, pad_v, hidden, carry,
     own_a, part_a, got_a, far_a, near_a, relay_a, fin_a,
     own_b, part_b, got_b, far_b, near_b, relay_b, fin_b,
-    final, stats, ssem, rsem, lsem,
+    final, stats, jumpt,
+    rgm, igm, rate, rtaps, spike, gtaps, vtaps, gain_r, gain_f, gain_c,
+    ssem, rsem, lsem,
 ):
     rep, fs, tp = lax.axis_index("rep"), lax.axis_index("fs"), lax.axis_index("tp")
     zlo, y = fs // NY, fs % NY
@@ -141,6 +141,10 @@
     loads = [pltpu.make_async_copy(stream, s_all.at[tp], lsem.at[6])]
     for i in range(6):
         loads.append(pltpu.make_async_copy(shards[i], wholes[i].at[zlo, y], lsem.at[i]))
+    far_small = (rgm_h, igm_h, rate_h, rtaps_h, spike_h, gtaps_h, vtaps_h, gain_r_h, gain_f_h, gain_c_h)
+    small = (rgm, igm, rate, rtaps, spike, gtaps, vtaps, gain_r, gain_f, gain_c)
+    for i in range(len(small)):
+        loads.append(pltpu.make_async_copy(far_small[i], small[i], lsem.at[7 + i]))
     for copy in loads:
         copy.start()
 
@@ -152,11 +156,11 @@
             pl.semaphore_signal(barrier, inc=1, device_id=friend, device_id_type=MESH)
         pl.semaphore_wait(barrier, len(friends))
     with scope("loads"):
-        for copy in loads:
+        for copy in loads[:7]:
             copy.wait()
 
     net = Net(ssem, rsem)
-    items = {}
+    items, ends = {}, []
 
     def item(name, deps, *args):
         def add(fn):
@@ -170,73 +174,69 @@
     def yslot(k):
         return (y + k + NY) % NY
 
-    def both(key, up_src, dn_src, line):
+    def both(i, key, up_src, dn_src, line):
         up, dn = (zup, zdn) if line == "z" else (yup, ydn)
-        net.send(key + "+", up_src, up_src, up, line + "+")
-        net.send(key + "-", dn_src, dn_src, dn, line + "-")
-
-    def landed(key):
-        net.take(key + "+", key + "-")
+        net.send(key, f"{i}{line}", up_src, up_src, up, line + "+")
+        net.send(key, f"{i}{line}", dn_src, dn_src, dn, line + "-")
 
     def coarse(i, g):
         n = f"w{i}."
         half = g.shape[2] // 2
-        steps = []
         if FIRST_Y[i]:
             steps = [
-                lambda: both(n + "0", g.at[zlo, y], g.at[zlo, y], "y"),
-                lambda: both(n + "1", g.at[zlo, yslot(-1), pl.ds(0, half)], g.at[zlo, yslot(1), pl.ds(half, half)], "y"),
-                lambda: both(n + "2", g.at[zlo], g.at[zlo], "z"),
-                lambda: both(n + "3", g.at[zslot(-1)], g.at[zslot(1)], "z"),
-                lambda: both(n + "4", g.at[zslot(-2)], g.at[zslot(2)], "z"),
-                lambda: both(n + "5", g.at[zslot(-3), pl.ds(0, 2)], g.at[zslot(3), pl.ds(2, 2)], "z"),
+                ("y", g.at[zlo, y], g.at[zlo, y], g.at[0, pl.ds(0, 2)]),
+                ("y", g.at[zlo, yslot(-1), pl.ds(0, half)], g.at[zlo, yslot(1), pl.ds(half, half)], g.at[0, 0]),
+                ("z", g.at[zlo], g.at[zlo], g.at[pl.ds(0, 2)]),
+                ("z", g.at[zslot(-1)], g.at[zslot(1)], g.at[pl.ds(0, 2)]),
+                ("z", g.at[zslot(-2)], g.at[zslot(2)], g.at[pl.ds(0, 2)]),
+                ("z", g.at[zslot(-3), pl.ds(0, 2)], g.at[zslot(3), pl.ds(2, 2)], g.at[0]),
             ]
         else:
             steps = [
-                lambda: both(n + "0", g.at[zlo, y], g.at[zlo, y], "z"),
-                lambda: both(n + "1", g.at[zslot(-1), y], g.at[zslot(1), y], "z"),
-                lambda: both(n + "2", g.at[zslot(-2), y], g.at[zslot(2), y], "z"),
-                lambda: both(n + "3", g.at[zslot(-3), y, pl.ds(0, half)], g.at[zslot(3), y, pl.ds(half, half)], "z"),
-                lambda: both(n + "4", g.at[:, y], g.at[:, y], "y"),
-                lambda: both(n + "5", g.at[pl.ds(0, 4), yslot(-1)], g.at[pl.ds(4, 4), yslot(1)], "y"),
+                ("z", g.at[zlo, y], g.at[zlo, y], g.at[0, pl.ds(0, 2)]),
+                ("z", g.at[zslot(-1), y], g.at[zslot(1), y], g.at[0, pl.ds(0, 2)]),
+                ("z", g.at[zslot(-2), y], g.at[zslot(2), y], g.at[0, pl.ds(0, 2)]),
+                ("z", g.at[zslot(-3), y, pl.ds(0, half)], g.at[zslot(3), y, pl.ds(half, half)], g.at[0, 0]),
+                ("y", g.at[:, y], g.at[:, y], g.at[pl.ds(0, 4)]),
+                ("y", g.at[pl.ds(0, 4), yslot(-1)], g.at[pl.ds(4, 4), yslot(1)], g.at[pl.ds(0, 2)]),
             ]
 
         def run(s):
             if s > 0:
-                landed(n + str(s - 1))
-            steps[s]()
+                net.take(n + str(s - 1), steps[s - 1][3])
+            if s < 6:
+                both(i, n + str(s), steps[s][1], steps[s][2], steps[s][0])
 
         for s in range(6):
             item(n + str(s), [n + str(s - 1)] if s else [], s)(run)
-        item(f"W{i}", [n + "5"])(lambda: landed(n + "5"))
+        item(f"W{i}", [n + "5"], 6)(run)
 
     def fine_y(i, g):
         n = f"w{i}."
         half = g.shape[2] // 2
-        item(n + "a", [])(lambda: both(n + "a", g.at[zlo, y], g.at[zlo, y], "y"))
+        two, one = g.at[0, pl.ds(0, 2)], g.at[0, 0]
+        item(n + "a", [])(lambda: both(i, n + "a", g.at[zlo, y], g.at[zlo, y], "y"))
 
         def relay():
-            landed(n + "a")
-            both(n + "b", g.at[zlo, yslot(-1), pl.ds(0, half)], g.at[zlo, yslot(1), pl.ds(half, half)], "y")
+            net.take(n + "a", two)
+            both(i, n + "b", g.at[zlo, yslot(-1), pl.ds(0, half)], g.at[zlo, yslot(1), pl.ds(half, half)], "y")
 
         item(n + "b", [n + "a"])(relay)
         before = ([], [n + "a"], [n + "a"], [n + "b"])
 
         def hop(j, o, k):
             if k == 0:
-                if j == 1:
-                    net.take(n + "a+")
-                elif j == 2:
-                    net.take(n + "a-")
+                if j in (1, 2):
+                    net.take(n + "a", two)
                 elif j == 3:
-                    landed(n + "b")
+                    net.take(n + "b", one)
             else:
-                landed(f"{n}{j}{k - 1}")
+                net.take(f"{n}{j}{k - 1}", two)
             yy = yslot(o)
             if k < 3:
-                both(f"{n}{j}{k}", g.at[zslot(-k), yy], g.at[zslot(k), yy], "z")
+                both(i, f"{n}{j}{k}", g.at[zslot(-k), yy], g.at[zslot(k), yy], "z")
             else:
-                both(f"{n}{j}{k}", g.at[zslot(-3), yy, pl.ds(0, half)], g.at[zslot(3), yy, pl.ds(half, half)], "z")
+                both(i, f"{n}{j}{k}", g.at[zslot(-3), yy, pl.ds(0, half)], g.at[zslot(3), yy, pl.ds(half, half)], "z")
 
         for j, o in enumerate((0, -1, 1, 2)):
             for k in range(4):
@@ -244,37 +244,36 @@
 
         def end():
             for j in range(4):
-                landed(f"{n}{j}3")
+                net.take(f"{n}{j}3", one)
 
         item(f"W{i}", [f"{n}{j}3" for j in range(4)] + [n + "b"])(end)
 
     def fine_z(i, g):
         n = f"w{i}."
         half = g.shape[2] // 2
+        two, one = g.at[0, pl.ds(0, 2)], g.at[0, 0]
 
         def hop(k):
             if k:
-                landed(f"{n}{k - 1}")
+                net.take(f"{n}{k - 1}", two)
             if k < 3:
-                both(f"{n}{k}", g.at[zslot(-k), y], g.at[zslot(k), y], "z")
+                both(i, f"{n}{k}", g.at[zslot(-k), y], g.at[zslot(k), y], "z")
             else:
-                both(f"{n}{k}", g.at[zslot(-3), y, pl.ds(0, half)], g.at[zslot(3), y, pl.ds(half, half)], "z")
+                both(i, f"{n}{k}", g.at[zslot(-3), y, pl.ds(0, half)], g.at[zslot(3), y, pl.ds(half, half)], "z")
 
         for k in range(4):
             item(f"{n}{k}", [f"{n}{k - 1}"] if k else [], k)(hop)
 
         def side(m, o):
             if o == 4:
-                landed(f"{n}3")
-            elif o < 0:
-                net.take(f"{n}{-o - 1}+")
-            elif o > 0:
-                net.take(f"{n}{o - 1}-")
-            both(f"{n}y{m}", g.at[zslot(o), y], g.at[zslot(o), y], "y")
+                net.take(f"{n}3", one)
+            elif o:
+                net.take(f"{n}{abs(o) - 1}", two)
+            both(i, f"{n}y{m}", g.at[zslot(o), y], g.at[zslot(o), y], "y")
 
         def relay(m, o):
-            landed(f"{n}y{m}")
-            both(f"{n}r{m}", g.at[zslot(o), yslot(-1), pl.ds(0, half)], g.at[zslot(o), yslot(1), pl.ds(half, half)], "y")
+            net.take(f"{n}y{m}", two)
+            both(i, f"{n}r{m}", g.at[zslot(o), yslot(-1), pl.ds(0, half)], g.at[zslot(o), yslot(1), pl.ds(half, half)], "y")
 
         ms = (0, -1, 1, -2, 2, -3, 3, 4)
         for m, o in enumerate(ms):
@@ -283,11 +282,15 @@
 
         def end():
             for m in range(8):
-                landed(f"{n}r{m}")
+                net.take(f"{n}r{m}", one)
 
         item(f"W{i}", [f"{n}r{m}" for m in range(8)])(end)
 
-    for i in range(6):
+    for i, g in enumerate(wholes):
+        if FIRST_Y[i]:
+            ends += [(f"{i}y", g.at[0, pl.ds(0, 3)]), (f"{i}z", g.at[pl.ds(0, 7)])]
+        else:
+            ends += [(f"{i}z", g.at[pl.ds(0, 7), 0]), (f"{i}y", g.at[pl.ds(0, 6)])]
         if FINE[i]:
             (fine_y if FIRST_Y[i] else fine_z)(i, wholes[i])
         else:
@@ -303,26 +306,30 @@
 
         def start():
             own = buf.at[tp, whole]
-            net.send(n + "0+", own, own, xup, "x+")
-            net.send(n + "0-", own, own, xdn, "x-")
-            net.send(n + "p0", own, own, pair, "d")
+            net.send(n + "0", n + "x", own, own, xup, "x+")
+            net.send(n + "0", n + "x", own, own, xdn, "x-")
+            net.send(n + "p", n + "p", own, own, pair, "d")
 
         def relay():
-            net.take(n + "0+")
-            net.send(n + "1+", buf.at[left, top], buf.at[left, top], xup, "x+")
-            net.take(n + "0-")
-            net.send(n + "1-", buf.at[right, low], buf.at[right, low], xdn, "x-")
-            net.send(n + "p1", buf.at[left, whole], buf.at[left, whole], pair, "d")
-            net.send(n + "p2", buf.at[right, whole], buf.at[right, whole], pair, "d")
+            net.take(n + "0", buf.at[pl.ds(0, 2), whole])
+            net.send(n + "1", n + "x", buf.at[left, top], buf.at[left, top], xup, "x+")
+            net.send(n + "1", n + "x", buf.at[right, low], buf.at[right, low], xdn, "x-")
+            net.send(n + "p", n + "p", buf.at[left, whole], buf.at[left, whole], pair, "d")
+            net.send(n + "p", n + "p", buf.at[right, whole], buf.at[right, whole], pair, "d")
 
         def last():
-            net.take(n + "1+", n + "1-")
-            net.send(n + "p3", buf.at[far, whole], buf.at[far, whole], pair, "d")
-
+            net.take(n + "1", buf.at[0, whole])
+            net.send(n + "p", n + "p", buf.at[far, whole], buf.at[far, whole], pair, "d")
+
+        def settle():
+            net.take(n + "p", buf.at[pl.ds(0, 4), whole])
+
+        ends.append((n + "x", buf.at[pl.ds(0, 3), whole]))
+        ends.append((n + "p", buf.at[pl.ds(0, 4), whole]))
         item(n + "0", deps)(start)
         item(n + "1", [n + "0"])(relay)
         item(n + "2", [n + "1"])(last)
-        item(n + "3", [n + "2"])(lambda: net.take(n + "p0", n + "p1", n + "p2", n + "p3"))
+        item(n + "3", [n + "2"])(settle)
 
     chunk = 32
 
@@ -344,7 +351,7 @@
         lax.fori_loop(0, size // chunk, body, 0)
         work(1.5 * size / 384)
 
-    def scatter(n, t, lhs, i, own, part, got, far, near, relay, fin, deps, finish):
+    def scatter(n, t, lhs, i, own, part, got, far, near, relay, fin, deps, finish, joint=False):
         g = wholes[i]
         lo = t * span
         top, low = slice(0, half_rows), slice(half_rows, span)
@@ -354,52 +361,72 @@
             xd = (x + o) % NX
             theirs = g[xd * NC + (1 - core)].reshape(NY * g.shape[2], g.shape[3])
             part[t, o] = nt(a, theirs).astype(BF16)
-            net.send(f"{n}d{o}", part.at[t, o], got.at[t, o], pair, "d")
+            net.send(f"{n}d{o % 2 or o}", n + "d", part.at[t, o], got.at[t, o], pair, "d")
             mine = g[xd * NC + core].reshape(NY * g.shape[2], g.shape[3])
             own[t, o] = nt(a, mine)
             work(0.4)
 
         def out_far():
-            net.take(n + "d2")
+            net.take(n + "d2", got.at[t, 2])
             far[t] = (own[t, 2] + got[t, 2].astype(F32)).astype(BF16)
             work(0.1)
-            net.send(n + "f+", far.at[t, pl.ds(0, half_rows)], relay.at[t, 0], xup, "x+")
-            net.send(n + "f-", far.at[t, pl.ds(half_rows, half_rows)], relay.at[t, 1], xdn, "x-")
+            net.send(n + "f", n + "f", far.at[t, pl.ds(0, half_rows)], relay.at[t, 0], xup, "x+")
+            net.send(n + "f", n + "f", far.at[t, pl.ds(half_rows, half_rows)], relay.at[t, 1], xdn, "x-")
 
         def out_near():
-            net.take(n + "d1", n + "d3")
+            net.take(n + "d1", got.at[t, pl.ds(0, 2)])
             near[t, 0, low, :] = (own[t, 1, low, :] + got[t, 1, low, :].astype(F32)).astype(BF16)
             near[t, 1, top, :] = (own[t, 3, top, :] + got[t, 3, top, :].astype(F32)).astype(BF16)
             work(0.1)
             at = pl.ds(half_rows, half_rows)
-            net.send(n + "n+", near.at[t, 0, at], fin.at[t, 0, at], xup, "x+")
+            net.send(n + "e", n + "e", near.at[t, 0, at], fin.at[t, 0, at], xup, "x+")
             at = pl.ds(0, half_rows)
-            net.send(n + "n-", near.at[t, 1, at], fin.at[t, 1, at], xdn, "x-")
+            net.send(n + "e", n + "e", near.at[t, 1, at], fin.at[t, 1, at], xdn, "x-")
 
         def out_relay():
-            net.take(n + "f+", n + "f-")
+            net.take(n + "f", relay.at[t])
             near[t, 0, top, :] = (own[t, 1, top, :] + got[t, 1, top, :].astype(F32) + relay[t, 0].astype(F32)).astype(BF16)
             near[t, 1, low, :] = (own[t, 3, low, :] + got[t, 3, low, :].astype(F32) + relay[t, 1].astype(F32)).astype(BF16)
             work(0.1)
             at = pl.ds(0, half_rows)
-            net.send(n + "r+", near.at[t, 0, at], fin.at[t, 0, at], xup, "x+")
+            net.send(n + "e", n + "e", near.at[t, 0, at], fin.at[t, 0, at], xup, "x+")
             at = pl.ds(half_rows, half_rows)
-            net.send(n + "r-", near.at[t, 1, at], fin.at[t, 1, at], xdn, "x-")
+            net.send(n + "e", n + "e", near.at[t, 1, at], fin.at[t, 1, at], xdn, "x-")
 
         def end():
-            net.take(n + "d0", n + "n+", n + "n-", n + "r+", n + "r-")
+            net.take(n + "d0", got.at[t, 0])
+            net.take(n + "e", fin.at[t])
             finish(own[t, 0] + got[t, 0].astype(F32) + fin[t, 0].astype(F32) + fin[t, 1].astype(F32))
 
-        for o in (2, 1, 3, 0):
-            item(f"{n}m{o}", deps, o)(mm)
-        item(n + "f", [n + "m2"])(out_far)
-        item(n + "n", [n + "m1", n + "m3"])(out_near)
+        ends.append((n + "d", part.at[t]))
+        ends.append((n + "f", far.at[t]))
+        ends.append((n + "e", near.at[t]))
+        def mm_joint(o):
+            a = lhs[...]
+            xd = (x + o) % NX
+            theirs = g[xd * NC + (1 - core)].reshape(NY * g.shape[2], g.shape[3])
+            terms = nt(a, theirs).astype(BF16)
+            for c in range(CHUNKS):
+                part[c, o] = terms[c * span : (c + 1) * span]
+                net.send(f"{n[0]}{c}d{o % 2 or o}", f"{n[0]}{c}d", part.at[c, o], got.at[c, o], pair, "d")
+            mine = g[xd * NC + core].reshape(NY * g.shape[2], g.shape[3])
+            terms = nt(a, mine)
+            for c in range(CHUNKS):
+                own[c, o] = terms[c * span : (c + 1) * span]
+            work(0.9)
+
+        m = n[0] + "m" if joint else n + "m"
+        if not joint or t == 0:
+            for o in (2, 1, 3, 0):
+                item(f"{m}{o}", deps, o)(mm_joint if joint else mm)
+        item(n + "f", [m + "2"])(out_far)
+        item(n + "n", [m + "1", m + "3"])(out_near)
         item(n + "r", [n + "f", n + "n"])(out_relay)
-        item(n + "e", [n + "r", n + "m0"])(end)
+        item(n + "e", [n + "r", m + "0"])(end)
 
     share("s", s_all, 0, rows, [])
     for t in range(2):
-        item(f"N{t}", ["s3"], s_all, gain_r, t * rows // 2, rows // 2)(norm_rows)
+        item(f"N{t}", ["s3", "L"], s_all, gain_r, t * rows // 2, rows // 2)(norm_rows)
 
     def weight(i, j=0, n=0):
         g = wholes[i]
@@ -419,6 +446,17 @@
     item("P1", ["N0", "N1", "W1"])(project_gate)
 
     heads, block = rgm.shape[0], rgm.shape[1]
+
+    def jump():
+        wide_rows = jnp.concatenate([spike[...], jnp.zeros((8 - heads, rows), F32)], axis=0)
+        jumpt[...] = wide_rows.T
+
+    def settled():
+        for copy in loads[7:]:
+            copy.wait()
+
+    item("L", [])(settled)
+    item("J", ["L"])(jump)
     piece = 64
 
     def recur(r):
@@ -433,7 +471,7 @@
             blk = conv[:, h * block : (h + 1) * block]
             reset.append(nn(blk, rgm[h]))
             admit.append(nn(blk, igm[h]))
-            jumps.append(jnp.broadcast_to(spike[lo : lo + piece, h : h + 1], (piece, block)))
+            jumps.append(jnp.broadcast_to(jumpt[lo : lo + piece, h : h + 1], (piece, block)))
         reset = sigmoid(jnp.concatenate(reset, axis=1))
         admit = sigmoid(jnp.concatenate(admit, axis=1))
         log_decay = -reset * base + jnp.concatenate(jumps, axis=1)
@@ -459,7 +497,7 @@
 
     per = span // piece
     for r in range(rows // piece):
-        item(f"R{r}", ["P0", "P1"] + ([f"R{r - 1}"] if r else []), r)(recur)
+        item(f"R{r}", ["P0", "P1", "J"] + ([f"R{r - 1}"] if r else []), r)(recur)
 
     def to_middle(t, total):
         at = slice(t * span, (t + 1) * span)
@@ -502,12 +540,11 @@
         sums = jnp.sum(lanes.T, axis=0, keepdims=True)
         stats[t, tp] = jnp.broadcast_to(sums, (8, span))
         work(0.5)
-        for k, device in enumerate(others):
-            net.send(f"q{t}{k}", stats.at[t, tp], stats.at[t, tp], device, "s")
+        for device in others:
+            net.send(f"q{t}", f"q{t}", stats.at[t, tp], stats.at[t, tp], device, "s")
 
     def finish(t):
-        for k in range(len(others)):
-            net.take(f"q{t}{k}")
+        net.take(f"q{t}", stats.at[t, pl.ds(0, 7)])
         at = slice(t * span, (t + 1) * span)
         total = stats[t, 0]
         for k in range(1, NX * NC):
@@ -528,8 +565,9 @@
             item(f"H{r}", ups + ([f"H{r - 1}"] if r else []), r)(mix)
         scatter(
             f"b{t}", t, hidden, 5, own_b, part_b, got_b, far_b, near_b, relay_b, fin_b,
-            ["W5"] + [f"H{t * per + q}" for q in range(per)], functools.partial(to_final, t),
+            ["W5"] + [f"H{q}" for q in range(rows // piece)], functools.partial(to_final, t), True,
         )
+        ends.append((f"q{t}", stats.at[t, pl.ds(0, 7)]))
         item(f"F{t}", [f"b{t}e"])(functools.partial(finish, t))
 
     emitted = set()
@@ -545,13 +583,18 @@
             fn()
         emitted.add(name)
 
-    for name in ORDER:
+    names = tuple(items)
+    for k in ORDER:
+        emit(names[k])
+    for name in names:
         emit(name)
-    for name in items:
-        emit(name)
+    LOG.append(("names", names))
     LOG.append(("item", "drain", tuple(items)))
     with scope("drain"):
-        net.drain()
+        for leave, ref in ends:
+            net.left(leave, ref)
+    assert not net.departures and set(net.arrivals) == net.taken, "unbalanced"
+    LOG.append(("counts", len(net.arrivals), len(ends)))
 
 
 def shards(
@@ -569,6 +612,11 @@
     wide = feedforward_gate_upward.shape[1]
     hbm = pl.BlockSpec(memory_space=pltpu.MemorySpace.HBM)
     vmem = pl.BlockSpec(memory_space=pltpu.VMEM)
+    small = (
+        recurrence_gate_matrix, input_gate_matrix, channel_decay_rate.reshape(1, -1), recurrence_taps,
+        spike_log_decay.T, feedforward_gate_taps, feedforward_value_taps,
+        recurrence_norm_gain.reshape(1, -1), feedforward_norm_gain.reshape(1, -1), closing_norm_gain.reshape(1, -1),
+    )
     span = rows // CHUNKS
     scatter = [
         pltpu.VMEM((CHUNKS, NX, span, cols), F32),
@@ -582,7 +630,7 @@
     return pl.pallas_call(
         layer_kernel,
         out_shape=jax.ShapeDtypeStruct((rows, cols), BF16),
-        in_specs=[hbm] * 7 + [vmem] * 10,
+        in_specs=[hbm] * 17,
         out_specs=vmem,
         scratch_shapes=[pltpu.VMEM((NZ, NY, *w.shape), BF16) for w in weights]
         + [
@@ -601,19 +649,20 @@
         + [
             pltpu.VMEM((rows, cols), F32),
             pltpu.VMEM((CHUNKS, tps, 8, span), F32),
-            pltpu.SemaphoreType.DMA((288,)),
-            pltpu.SemaphoreType.DMA((288,)),
-            pltpu.SemaphoreType.DMA((7,)),
+            pltpu.VMEM((rows, 8), F32),
+        ]
+        + [pltpu.VMEM(v.shape, v.dtype) for v in small]
+        + [
+            pltpu.SemaphoreType.DMA((32,)),
+            pltpu.SemaphoreType.DMA((SEMS,)),
+            pltpu.SemaphoreType.DMA((17,)),
         ],
         compiler_params=pltpu.CompilerParams(
             collective_id=0, has_side_effects=True, vmem_limit_bytes=60 * 1024 * 1024
         ),
         name="layer",
     )(
-        stream, *weights,
-        recurrence_gate_matrix, input_gate_matrix, channel_decay_rate.reshape(1, -1), recurrence_taps,
-        spike_log_decay, feedforward_gate_taps, feedforward_value_taps,
-        recurrence_norm_gain.reshape(1, -1), feedforward_norm_gain.reshape(1, -1), closing_norm_gain.reshape(1, -1),
+        stream, *weights, *small,
     )
 
 

time: 112 us -> 89.3 us (0.80)
  Pallas kernels: 108 us -> 87.6 us
  local copies, waits for them, and re-layouts: 3.12 us -> 1.62 us
    pallas_call x1, Pallas kernels: 108 us -> 87.6 us  [shards(): pl.pallas_call(layer_kernel, out_shape=jax.ShapeDtypeStruct((rows, cols),...]
    unnamed x4 -> x1, local copies, waits for them, and re-layouts: 3.12 us -> 1.62 us
where the time goes in v3:
time: 89.3 us; the launch traced here: 89.2 us
  Pallas kernels  87.6 us (98%)
  local copies, waits for them, and re-layouts  1.62 us (2%)
    pallas_call x1, Pallas kernels, shards(): pl.pallas_call(layer_kernel, out_shape=jax.ShapeDtypeStruct((rows, cols),...  87.6 us

profile of v3, /device:TPU:1, one launch (start us, length us, event | category | flops | bytes accessed | tf_op | source)
XLA Modules:
  0.0 89.2 jit_solution(12608561448271494086)
XLA Ops:
  0.0 87.6 %layer.1 = bf16[384,256]{1,0:T(8,128)(2,1)} custom-call(bf16[384,256]{1,0:T(8,128)(2,1)} %stream.1, bf16[64,256]{1,0:T(8,128)(2,1)} %w_in.1, bf16[64,256]{1,0:T(8,128)(2,1)} %w_gate.1, bf16[64,256]{1,0:T(8,128)(2,1)} %bitcast.8, bf16[64,512]{1,0:T(8,128)(2,1)} %w_fg.1, bf16[64,512]{1,0:T(8,128)(2,1)} %w_fv.1, bf16[64,512]{1,0:T(8,128)(2,1)} %bitcast.7, ...), custom_call_target="tpu_custom_call" | custom-call | tf_op jit(solution)/shard_map/layer/pallas_call | solution.py:630
  87.6 1.6 %copy.19 = bf16[384,256]{1,0:T(8,128)(2,1)} copy(bf16[384,256]{1,0:T(8,128)(2,1)} %layer.1) | data formatting | bytes 393216

commit v4 on v3

--- a/solution.py
+++ b/solution.py
@@ -20,15 +20,15 @@
 SEMS = 145
 LOG = []
 ORDER = (
-    42, 40, 0, 19, 120, 128, 129, 2, 23, 59, 63, 80, 101, 46, 1, 41, 20, 24, 27, 10, 65, 6,
-    121, 3, 86, 14, 47, 31, 21, 29, 54, 28, 7, 66, 11, 25, 122, 15, 64, 4, 32, 33, 123, 124,
-    22, 35, 50, 125, 8, 30, 84, 12, 16, 26, 43, 102, 55, 37, 51, 36, 34, 9, 67, 13, 5, 17,
-    48, 85, 44, 87, 56, 38, 88, 52, 81, 18, 126, 68, 49, 45, 39, 127, 53, 57, 130, 60, 89, 131,
-    132, 82, 92, 133, 134, 135, 115, 90, 58, 149, 151, 150, 71, 61, 152, 153, 136, 69, 138, 154, 83, 139,
-    94, 107, 137, 140, 103, 96, 155, 141, 62, 72, 111, 73, 142, 108, 70, 156, 157, 75, 116, 77, 104, 143,
-    144, 74, 112, 95, 97, 158, 109, 76, 98, 117, 145, 78, 105, 93, 159, 91, 113, 160, 161, 146, 110, 99,
-    118, 79, 178, 179, 106, 147, 148, 162, 114, 163, 100, 181, 164, 180, 165, 166, 167, 168, 119, 182, 183, 184,
-    169, 171, 173, 170, 185, 172, 174, 186, 175, 187, 176, 188, 177, 189,
+    42, 0, 101, 120, 19, 2, 59, 84, 10, 1, 23, 40, 20, 25, 3, 80, 11, 14, 65, 29, 41, 27,
+    6, 26, 46, 121, 86, 50, 21, 24, 15, 30, 102, 12, 43, 31, 7, 22, 122, 4, 28, 33, 63, 54,
+    51, 16, 35, 128, 123, 32, 129, 47, 8, 37, 67, 34, 55, 13, 52, 36, 124, 17, 5, 38, 9, 44,
+    48, 56, 81, 66, 88, 125, 39, 127, 53, 18, 87, 45, 126, 49, 130, 57, 64, 85, 60, 68, 131, 132,
+    133, 92, 82, 111, 134, 135, 58, 136, 90, 138, 89, 69, 61, 71, 149, 137, 94, 115, 83, 96, 140, 103,
+    150, 151, 112, 141, 139, 142, 62, 72, 73, 152, 153, 116, 107, 75, 143, 144, 77, 104, 98, 154, 117, 70,
+    74, 108, 93, 76, 113, 145, 155, 78, 99, 105, 91, 95, 97, 109, 146, 156, 157, 114, 118, 79, 147, 148,
+    159, 106, 158, 110, 100, 160, 161, 162, 163, 164, 174, 175, 176, 119, 165, 167, 169, 166, 177, 170, 168, 178,
+    171, 179, 172, 180, 173, 181,
 )
 
 
@@ -413,7 +413,7 @@
             terms = nt(a, mine)
             for c in range(CHUNKS):
                 own[c, o] = terms[c * span : (c + 1) * span]
-            work(0.9)
+            work(0.4 + g.shape[3] / 1024)
 
         m = n[0] + "m" if joint else n + "m"
         if not joint or t == 0:
@@ -507,19 +507,17 @@
     for t in range(CHUNKS):
         scatter(
             f"a{t}", t, mixed, 2, own_a, part_a, got_a, far_a, near_a, relay_a, fin_a,
-            ["W2"] + [f"R{t * per + q}" for q in range(per)], functools.partial(to_middle, t),
+            ["W2"] + [f"R{q}" for q in range(rows // piece)], functools.partial(to_middle, t), True,
         )
         share(f"m{t}", m_all, t * span, span, [f"a{t}e"])
         item(f"M{t}", [f"m{t}3", "P0", "P1"], m_all, gain_f, t * span, span)(norm_rows)
 
     wide = g_fg.shape[3]
 
-    def up(t, i, pad, j):
-        at = slice(t * span, (t + 1) * span)
-        if t == 0:
-            pad[0:8, j : j + 256] = jnp.zeros((8, 256), F32)
-        pad[8 + t * span : 8 + (t + 1) * span, j : j + 256] = nn(normed[at, :], weight(i, j, 256)).astype(BF16).astype(F32)
-        work(0.6)
+    def up(i, pad, j):
+        pad[0:8, j : j + 256] = jnp.zeros((8, 256), F32)
+        pad[8:, j : j + 256] = nn(normed[...], weight(i, j, 256)).astype(BF16).astype(F32)
+        work(0.95)
 
     def mix(r):
         lo = r * piece
@@ -554,12 +552,12 @@
         out[at, :] = (final[at, :] * inverse * gain).astype(BF16)
         work(0.4)
 
+    ups = []
+    for i, pad in ((3, pad_g), (4, pad_v)):
+        for j in range(0, wide, 256):
+            ups.append(f"u{i}{j // 256}")
+            item(ups[-1], [f"M{t}" for t in range(CHUNKS)] + [f"W{i}"], i, pad, j)(up)
     for t in range(CHUNKS):
-        ups = []
-        for i, pad in ((3, pad_g), (4, pad_v)):
-            for j in range(0, wide, 256):
-                ups.append(f"u{t}{i}{j // 256}")
-                item(ups[-1], [f"M{t}", f"W{i}"], t, i, pad, j)(up)
         for q in range(per):
             r = t * per + q
             item(f"H{r}", ups + ([f"H{r - 1}"] if r else []), r)(mix)

time: 89.3 us -> 92 us (1.030)
  Pallas kernels: 87.6 us -> 90.3 us
    pallas_call x1, Pallas kernels: 87.6 us -> 90.3 us  [shards(): pl.pallas_call(layer_kernel, out_shape=jax.ShapeDtypeStruct((rows, cols),...]
where the time goes in v4:
time: 92 us; the launch traced here: 91.9 us
  Pallas kernels  90.3 us (98%)
  local copies, waits for them, and re-layouts  1.62 us (2%)
    pallas_call x1, Pallas kernels, shards(): pl.pallas_call(layer_kernel, out_shape=jax.ShapeDtypeStruct((rows, cols),...  90.3 us

profile of v4, /device:TPU:1, one launch (start us, length us, event | category | flops | bytes accessed | tf_op | source)
XLA Modules:
  0.0 91.9 jit_solution(7793543616541181562)
XLA Ops:
  0.0 90.3 %layer.1 = bf16[384,256]{1,0:T(8,128)(2,1)} custom-call(bf16[384,256]{1,0:T(8,128)(2,1)} %stream.1, bf16[64,256]{1,0:T(8,128)(2,1)} %w_in.1, bf16[64,256]{1,0:T(8,128)(2,1)} %w_gate.1, bf16[64,256]{1,0:T(8,128)(2,1)} %bitcast.8, bf16[64,512]{1,0:T(8,128)(2,1)} %w_fg.1, bf16[64,512]{1,0:T(8,128)(2,1)} %w_fv.1, bf16[64,512]{1,0:T(8,128)(2,1)} %bitcast.7, ...), custom_call_target="tpu_custom_call" | custom-call | tf_op jit(solution)/shard_map/layer/pallas_call | solution.py:628
  90.3 1.6 %copy.19 = bf16[384,256]{1,0:T(8,128)(2,1)} copy(bf16[384,256]{1,0:T(8,128)(2,1)} %layer.1) | data formatting | bytes 393216
